TPU v7x, 256 devices: a whole 4x4x8 slice. The times are simulated.
256 devices in a mesh: ra: 16 (over y, x), cb: 16 (over z, core).
Axes of the slice: x: 4, y: 4, z: 8, core: 2. Of those that a mesh axis runs over, the one named last changes fastest.
Arguments:
- tokens: bfloat16 [512, 4096], P(None, 'ra'), may hold values from -40 to 40, as said below
- norm_gain: float32 [2, 4096], P(None, 'ra'), may hold values from 0.1 to 1.9
- gate_weight: bfloat16 [2, 4096, 11264], P(None, 'ra', 'cb'), may hold values from -0.09375 to 0.09375
- up_weight: bfloat16 [2, 4096, 11264], P(None, 'ra', 'cb'), may hold values from -0.09375 to 0.09375
- down_weight: bfloat16 [2, 11264, 4096], P(None, 'cb', 'ra'), may hold values from -0.0546875 to 0.0546875
Outputs:
- result: bfloat16 [512, 4096], P(None, 'ra')
Inputs may be any that keep to these rules, and one draw needn't show every extreme that they name: `tokens`: features come in blocks of 32 with scales that differ from block to block by up to a factor of 16.
All inputs are finite; a program needn't handle non-finite values.
Results may differ from a plain program's by a relative error of at most 0.0075.
Values may be sent and summed in bfloat16 or wider, within the bound.
A program may use at most 64 MiB of HBM per device.

v0:
```python
import functools

import jax
import jax.numpy as jnp
from jax import lax
from jax.sharding import Mesh
from jax.sharding import PartitionSpec as P

D = 4096
LAYERS = 2
RA = ("ra_0", "ra_1")


epsilon = 1e-06
keep_share = 0.5


def over_axes(array, axes):
    return functools.reduce(lax.psum, axes, array)


def in_blocks(array, dim, size):
    shape = array.shape
    blocks = array.reshape(*shape[:dim], size, shape[dim] // size, *shape[dim + 1 :])
    return jnp.moveaxis(blocks, dim, 0)


def sent_and_summed(array, axis, dim):
    size = lax.axis_size(axis)
    blocks = lax.all_to_all(in_blocks(array, dim, size), axis, 0, 0, tiled=True)
    return jnp.sum(blocks, axis=0)


def in_one_piece(arrays, axis, dim, along):
    ends, at = ([], 0)
    for a in arrays[:-1]:
        at += a.shape[along]
        ends.append(at)
    both = jnp.concatenate(arrays, axis=along)
    return tuple(jnp.split(sent_and_summed(both, axis, dim), ends, axis=along))


def copy_for_each(array, axis):
    copies = jnp.broadcast_to(array, (lax.axis_size(axis), *array.shape))
    return lax.all_to_all(copies, axis, split_axis=0, concat_axis=0, tiled=True)


def joined_along(blocks, dim):
    blocks = jnp.moveaxis(blocks, 0, dim)
    shape = blocks.shape
    return blocks.reshape(*shape[:dim], shape[dim] * shape[dim + 1], *shape[dim + 2 :])


def gather_directly(array, axis, dim):
    blocks = copy_for_each(array, axis)
    return joined_along(blocks, dim)


def gathered_total(array, axis):
    blocks = lax.all_gather(array, axis)
    return blocks.sum(axis=0)


def body(tokens, norm_gain, gate_weight, up_weight, down_weight):
    stream = tokens
    for layer in range(LAYERS):
        widened = stream.astype(jnp.float32)
        squares = jnp.sum(widened * widened, axis=1)
        normed = (widened * norm_gain[layer]).astype(jnp.bfloat16)
        gate_part = jnp.dot(normed, gate_weight[layer], preferred_element_type=jnp.float32)
        up_part = jnp.dot(normed, up_weight[layer], preferred_element_type=jnp.float32)
        total = over_axes(squares, RA)
        gate_share, up_share = in_one_piece((gate_part, up_part), RA, 1, 0)
        scale = lax.rsqrt(total / D + epsilon)[:, None]
        share = (jax.nn.silu(gate_share * scale) * (up_share * scale)).astype(jnp.bfloat16)
        hidden = gather_directly(share, RA, 1)
        partial_down = jnp.dot(hidden, down_weight[layer], preferred_element_type=jnp.float32)
        branch = gathered_total(partial_down, "cb")
        stream = (keep_share * widened + branch).astype(jnp.bfloat16)
    return stream


def solution(mesh):
    torus = Mesh(mesh.devices.reshape(4, 4, mesh.shape["cb"]), ("ra_0", "ra_1", "cb"))
    in_specs = (P(None, RA), P(None, RA), P(None, RA, "cb"), P(None, RA, "cb"), P(None, "cb", RA))
    out_specs = P(None, RA)
    return jax.shard_map(body, mesh=torus, in_specs=in_specs, out_specs=out_specs, check_vma=False)
```

profile of v0, /device:TPU:1, one launch (start us, length us, event | category | flops | bytes accessed | tf_op | source)
XLA Modules:
  0.0 290.1 jit_solution(14399984629574766054)
XLA Ops:
  6.5 0.8 fusion.35
  7.3 1.4 fusion.16
  8.7 1.4 fusion.18
  10.5 1.8 reshape.14
  12.3 7.7 %all-to-all-start = ((f32[16,1024,44]{1,2,0:T(8,128)}), f32[16,1024,44]{1,2,0:T(8,128)S(1)}, u32[]{:S(2)}, u32[]{:S(2)}) async-start(f32[16,1024,44]{1,2,0:T(8,128)} %bitcast.36), calls=%async_computation | async-start | bytes 6291456 | tf_op jit(solution)/shard_map/all_to_all | solution.py:30
  20.2 27.5 %psum.28 = f32[512]{0:T(512)S(1)} all-reduce(f32[512]{0:T(512)S(1)} %fusion.3), channel_id=1, replica_groups=mesh['ra_0'=4,'ra_1'=4,'cb'=16] {'ra_0'}, use_global_device_ids=true, to_apply=%region_2.0 | all-reduce | flops 512 | bytes 4096 | tf_op jit(solution)/shard_map/psum | solution.py:19
  47.7 19.5 %psum.29 = f32[512]{0:T(512)S(1)} all-reduce(f32[512]{0:T(512)S(1)} %psum.28), channel_id=1, replica_groups=mesh['ra_0'=4,'ra_1'=4,'cb'=16] {'ra_1'}, use_global_device_ids=true, to_apply=%region_3.0 | all-reduce | flops 512 | bytes 4096 | tf_op jit(solution)/shard_map/psum | solution.py:19
  67.2 0.9 reduce_sum.54
  68.1 1.0 fusion.33
  69.2 15.3 %all_to_all.20 = bf16[16,512,44]{1,2,0:T(8,128)(2,1)S(1)} all-to-all(bf16[16,512,44]{1,2,0:T(8,128)(2,1)S(1)} %broadcast_in_dim.8), channel_id=1, replica_groups=mesh['ra_0'=4,'ra_1'=4,'cb'=16] {'ra_0','ra_1'}, dimensions={0} | all-to-all | bytes 1441792 | tf_op jit(solution)/shard_map/all_to_all | solution.py:45
  84.7 1.3 fusion.14
  85.9 58.6 %all-gather.5.cloned.1.call-done = f32[8192,256]{1,0:T(8,128)} async-done(((f32[512,256]{1,0:T(8,128)}), f32[8192,256]{1,0:T(8,128)}) %all-gather.5.cloned.1.call-update) | async-done | bytes 8388624 | tf_op jit(solution)/shard_map/all_gather | solution.py:60
  144.5 4.0 %reduce_sum.56 = f32[512,256]{1,0:T(8,128)S(1)} reduce(f32[16,512,256]{2,1,0:T(8,128)} %bitcast.39, f32[]{:T(128)} %constant.10.clone.1), dimensions={0}, to_apply=%region_4.5 | reduce | flops 1966080 | bytes 8912900 | tf_op jit(solution)/shard_map/reduce_sum | solution.py:61
  148.8 0.4 fusion.12
  149.7 0.4 fusion.10
  150.4 1.8 reshape.16
  152.2 6.5 %all-to-all-start.2 = ((f32[16,1024,44]{1,2,0:T(8,128)}), f32[16,1024,44]{1,2,0:T(8,128)S(1)}, u32[]{:S(2)}, u32[]{:S(2)}) async-start(f32[16,1024,44]{1,2,0:T(8,128)} %bitcast.37), calls=%async_computation.2 | async-start | bytes 6291456 | tf_op jit(solution)/shard_map/all_to_all | solution.py:30
  158.8 27.8 %psum.30 = f32[512]{0:T(512)S(1)} all-reduce(f32[512]{0:T(512)S(1)} %get-tuple-element.5), channel_id=1, replica_groups=mesh['ra_0'=4,'ra_1'=4,'cb'=16] {'ra_0'}, use_global_device_ids=true, to_apply=%region_7.8 | all-reduce | flops 512 | bytes 4096 | tf_op jit(solution)/shard_map/psum | solution.py:19
  186.6 20.6 %psum.31 = f32[512]{0:T(512)S(1)} all-reduce(f32[512]{0:T(512)S(1)} %psum.30), channel_id=1, replica_groups=mesh['ra_0'=4,'ra_1'=4,'cb'=16] {'ra_1'}, use_global_device_ids=true, to_apply=%region_8.9 | all-reduce | flops 512 | bytes 4096 | tf_op jit(solution)/shard_map/psum | solution.py:19
  207.6 15.6 %all_to_all.21 = bf16[16,512,44]{1,2,0:T(8,128)(2,1)S(1)} all-to-all(bf16[16,512,44]{1,2,0:T(8,128)(2,1)S(1)} %broadcast_in_dim.9), channel_id=1, replica_groups=mesh['ra_0'=4,'ra_1'=4,'cb'=16] {'ra_0','ra_1'}, dimensions={0} | all-to-all | bytes 1441792 | tf_op jit(solution)/shard_map/all_to_all | solution.py:45
  223.3 1.3 fusion.8
  224.6 53.9 %all-gather.7.cloned.1.call-done = f32[8192,256]{1,0:T(8,128)} async-done(((f32[512,256]{1,0:T(8,128)}), f32[8192,256]{1,0:T(8,128)}) %all-gather.7.cloned.1.call-update) | async-done | bytes 8388624 | tf_op jit(solution)/shard_map/all_gather | solution.py:60
  278.5 4.0 %reduce_sum.59 = f32[512,256]{1,0:T(8,128)S(1)} reduce(f32[16,512,256]{2,1,0:T(8,128)} %bitcast.38, f32[]{:T(128)} %constant.10.clone.1), dimensions={0}, to_apply=%region_9.10 | reduce | flops 1966080 | bytes 8912900 | tf_op jit(solution)/shard_map/reduce_sum | solution.py:61
  282.5 0.8 fusion.5
  (32 shorter events, 2.2 us)
Async XLA Ops:
  12.3 7.8 %copy-start = (bf16[512,256]{1,0:T(8,128)(2,1)S(1)}, bf16[512,256]{1,0:T(8,128)(2,1)}, u32[]{:S(2)}) copy-start(bf16[512,256]{1,0:T(8,128)(2,1)} %param.5) | copy-start | bytes 786436
  12.3 54.9 %all-to-all-start = ((f32[16,1024,44]{1,2,0:T(8,128)}), f32[16,1024,44]{1,2,0:T(8,128)S(1)}, u32[]{:S(2)}, u32[]{:S(2)}) async-start(f32[16,1024,44]{1,2,0:T(8,128)} %bitcast.36), calls=%async_computation | async-start | bytes 6291456 | tf_op jit(solution)/shard_map/all_to_all | solution.py:30
  20.0 124.5 %all-gather.5.cloned.1.call-start = ((), (), s32[]{:S(2)}) async-start(), calls=%async_computation.4 | async-start | bytes 8912896 | tf_op jit(solution)/shard_map/all_gather | solution.py:60
  68.1 16.6 %copy-start.5 = (bf16[2,704,256]{2,1,0:T(8,128)(2,1)S(1)}, bf16[2,704,256]{2,1,0:T(8,128)(2,1)}, u32[]{:S(2)}) copy-start(bf16[2,704,256]{2,1,0:T(8,128)(2,1)} %param.9) | copy-start | bytes 2162692
  144.5 4.2 %copy-start.3 = (bf16[2,256,704]{1,2,0:T(8,128)(2,1)S(1)}, bf16[2,256,704]{1,2,0:T(8,128)(2,1)}, u32[]{:S(2)}) copy-start(bf16[2,256,704]{1,2,0:T(8,128)(2,1)} %param.7) | copy-start | bytes 2162692
  148.6 1.2 copy-start.4
  148.7 0.7 copy-start.1
  152.2 55.0 %all-to-all-start.2 = ((f32[16,1024,44]{1,2,0:T(8,128)}), f32[16,1024,44]{1,2,0:T(8,128)S(1)}, u32[]{:S(2)}, u32[]{:S(2)}) async-start(f32[16,1024,44]{1,2,0:T(8,128)} %bitcast.37), calls=%async_computation.2 | async-start | bytes 6291456 | tf_op jit(solution)/shard_map/all_to_all | solution.py:30
  158.7 119.8 %all-gather.7.cloned.1.call-start = ((), (), s32[]{:S(2)}) async-start(), calls=%async_computation.5 | async-start | bytes 8912896 | tf_op jit(solution)/shard_map/all_gather | solution.py:60
  207.4 15.9 %copy-start.6 = (bf16[2,704,256]{2,1,0:T(8,128)(2,1)S(1)}, bf16[2,704,256]{2,1,0:T(8,128)(2,1)}, u32[]{:S(2)}) copy-start(bf16[2,704,256]{2,1,0:T(8,128)(2,1)} %param.9) | copy-start | bytes 2162692
  278.5 4.0 %copy-start.2 = (bf16[512,256]{1,0:T(8,128)(2,1)S(1)}, bf16[512,256]{1,0:T(8,128)(2,1)}, u32[]{:S(2)}) copy-start(bf16[512,256]{1,0:T(8,128)(2,1)} %copy-done.1) | copy-start | bytes 786436
Sparse Core Ops, SparseCore 0:
  86.1 58.4 all-gather.4
  224.7 53.7 all-gather.6
where the time goes:
time: 291 us; the launch traced here: 290 us
  blocking collectives  126 us (43%)
  waiting for transfers between devices  112 us (38%)
  starting transfers between devices  14.3 us (5%)
  between operations  13.6 us (5%)
  other arithmetic  11.9 us (4%)
  matrix products  6.18 us (2%)
  local copies, waits for them, and re-layouts  5.42 us (2%)
    all_gather x2, waiting for transfers between devices, gathered_total(): blocks = lax.all_gather(array, axis)  112 us
    psum x4, blocking collectives, over_axes(): return functools.reduce(lax.psum, axes, array)  95.4 us
    all_to_all x2, blocking collectives, copy_for_each(): return lax.all_to_all(copies, axis, split_axis=0, concat_axis=0, tiled=True)  30.9 us
    all_to_all x2, starting transfers between devices, sent_and_summed(): blocks = lax.all_to_all(in_blocks(array, dim, size), axis, 0, 0, tiled=True)  14.2 us
    reduce_sum x2, other arithmetic, gathered_total(): return blocks.sum(axis=0)  8.06 us
  transfers between devices with their start and end apart: 4, of which 2 were waited for; matrix products, arithmetic and copies ran while one was open for 0% of the time, Pallas kernels for 0%

commit v1 on v0

v1 whole, which is shorter than its diff:
```python
import functools

import jax
import jax.numpy as jnp
from jax import lax
from jax.experimental import pallas as pl
from jax.experimental.pallas import tpu as pltpu
from jax.sharding import Mesh
from jax.sharding import PartitionSpec as P

MESH = pl.DeviceIdType.MESH
LAYERS = 2
EPSILON = 1e-06
KEEP = 0.5
F32 = jnp.float32
BF16 = jnp.bfloat16


def far_first(n):
    return sorted(range(1, n), key=lambda d: (-min(d, n - d), d))


def kernel(n, nz, features, tok, gain, wg, wu, wd, out, *scratch):
    (
        stream, gains, graw, uraw, wcat, down,
        send1, recv1, own1, send2, recv2, own2, hid, part, send3, recv3,
        load_sem, peer_sem, s1, r1, s2, r2, s3, r3, s4, r4, s5, r5, s6, r6, s7, r7,
    ) = scratch
    y, x, z, c = (lax.axis_index(a) for a in ("y", "x", "z", "c"))
    half = stream.shape[1] * stream.shape[2]
    group = half // n
    rows = group // n
    zrows = half // nz
    width = wg.shape[2]
    p = c * x + (1 - c) * y
    q = c * y + (1 - c) * x

    def p_peer(d):
        return {"y": lax.rem(y + (1 - c) * d, n), "x": lax.rem(x + c * d, n)}

    def q_peer(d):
        return {"y": lax.rem(y + c * d, n), "x": lax.rem(x + (1 - c) * d, n)}

    def z_peer(d):
        return {"z": lax.rem(z + d, nz)}

    other = {"c": 1 - c}
    pending = []

    def send(src, dst, ss, rs, to):
        copy = pltpu.make_async_remote_copy(src, dst, ss, rs, device_id=to, device_id_type=MESH)
        copy.start()
        pending.append(copy)
        return copy

    barrier = pltpu.get_barrier_semaphore()
    greeted = [p_peer(d) for d in range(1, n)] + [q_peer(d) for d in range(1, n)]
    greeted += [z_peer(d) for d in range(1, nz)] + [other]
    for peer in greeted:
        pl.semaphore_signal(barrier, 1, device_id=peer, device_id_type=MESH)

    loads = [
        pltpu.make_async_copy(wg.at[0], graw.at[0, 0], load_sem.at[0]),
        pltpu.make_async_copy(wu.at[0], uraw.at[0, 0], load_sem.at[1]),
        pltpu.make_async_copy(gain, gains, load_sem.at[2]),
        pltpu.make_async_copy(wg.at[1], graw.at[1, 0], load_sem.at[3]),
        pltpu.make_async_copy(wu.at[1], uraw.at[1, 0], load_sem.at[4]),
        pltpu.make_async_copy(wd.at[0], down.at[0, 0], load_sem.at[5]),
        pltpu.make_async_copy(wd.at[1], down.at[1, 0], load_sem.at[6]),
    ]
    token_loads = [
        pltpu.make_async_copy(tok.at[pl.ds(c * half + k * zrows, zrows)], stream.at[0, k], load_sem.at[7 + k])
        for k in range(nz)
    ]
    for copy in token_loads + loads:
        copy.start()
    for copy in token_loads + loads[:3]:
        copy.wait()

    def join(layer, block):
        wcat[layer, block] = jnp.concatenate([graw[layer, block], uraw[layer, block]], axis=1)

    join(0, 0)
    pl.semaphore_wait(barrier, len(greeted))
    from_peer = []
    for layer in range(LAYERS):
        from_peer.append([
            send(wg.at[layer], graw.at[layer, 1], peer_sem.at[0, layer, 0], peer_sem.at[1, layer, 0], other),
            send(wu.at[layer], uraw.at[layer, 1], peer_sem.at[0, layer, 1], peer_sem.at[1, layer, 1], other),
            send(wd.at[layer], down.at[layer, 1], peer_sem.at[0, layer, 2], peer_sem.at[1, layer, 2], other),
        ])

    first_half = lax.broadcasted_iota(jnp.int32, (1, 128), 1) < 64

    def two_parts(total):
        high = total.astype(BF16).astype(F32)
        return jnp.where(first_half, high, total - high)

    def whole(parts):
        return parts + pltpu.roll(parts, 64, 1)

    for layer in range(LAYERS):
        in_flight = {}
        for block in range(2):
            if block == 1:
                for copy in from_peer[layer][:2]:
                    copy.wait_recv()
                join(layer, 1)
            elif layer > 0:
                for copy in loads[3:5]:
                    copy.wait()
                join(layer, 0)
            for d in far_first(n) + [0]:
                to = lax.rem(p + d, n)
                tokens = stream[layer, pl.ds(to * (nz // n), nz // n)].reshape(group, -1).astype(F32)
                normed = (tokens * gains[pl.ds(layer, 1)]).astype(BF16)
                product = jnp.dot(normed, wcat[layer, block], preferred_element_type=F32)
                if block == 0:
                    squares = jnp.sum(tokens * tokens, axis=1, keepdims=True)
                    squares = jnp.broadcast_to(squares, (group, 128))
                if d == 0:
                    own1[layer, block, :, : 2 * width] = product
                    if block == 0:
                        own1[layer, 0, :, 2 * width :] = jnp.where(first_half, squares, 0.0)
                else:
                    send1[layer, block, d - 1, :, : 2 * width] = product.astype(BF16)
                    if block == 0:
                        send1[layer, 0, d - 1, :, 2 * width :] = two_parts(squares).astype(BF16)
                    span = slice(None) if block == 0 else pl.ds(0, 2 * width)
                    in_flight[block, d] = send(
                        send1.at[layer, block, d - 1, :, span],
                        recv1.at[layer, block, d - 1, :, span],
                        s1.at[layer, block, d - 1],
                        r1.at[layer, block, d - 1],
                        p_peer(d),
                    )
        second = {}
        for block in range(2):
            for d in range(1, n):
                in_flight[block, d].wait_recv()
            w = 2 * width + 128 if block == 0 else 2 * width
            for d in far_first(n) + [0]:
                mine = pl.ds(pl.multiple_of(lax.rem(q + d, n) * rows, rows), rows)
                total = own1[layer, block, mine, :w]
                for e in range(n - 1):
                    total = total + recv1[layer, block, e, mine, :w].astype(F32)
                if block == 0:
                    squares = whole(total[:, 2 * width :])
                    total = total[:, : 2 * width]
                if d == 0:
                    own2[layer, block, :, : 2 * width] = total
                    if block == 0:
                        own2[layer, 0, :, 2 * width :] = jnp.where(first_half, squares, 0.0)
                else:
                    send2[layer, block, d - 1, :, : 2 * width] = total.astype(BF16)
                    if block == 0:
                        send2[layer, 0, d - 1, :, 2 * width :] = two_parts(squares).astype(BF16)
                    span = slice(None) if block == 0 else pl.ds(0, 2 * width)
                    second[block, d] = send(
                        send2.at[layer, block, d - 1, :, span],
                        recv2.at[layer, block, d - 1, :, span],
                        s2.at[layer, block, d - 1],
                        r2.at[layer, block, d - 1],
                        q_peer(d),
                    )
        shares = []
        for block in range(2):
            for d in range(1, n):
                second[block, d].wait_recv()
            w = 2 * width + 128 if block == 0 else 2 * width
            total = own2[layer, block, :, :w]
            for e in range(n - 1):
                total = total + recv2[layer, block, e, :, :w].astype(F32)
            if block == 0:
                squares = whole(total[:, 2 * width :])
                scale = lax.rsqrt(squares[:, :1] / features + EPSILON)
            gate = total[:, :width] * scale
            up = total[:, width : 2 * width] * scale
            shares.append(gate / (1.0 + jnp.exp(-gate)) * up)
        hid[layer, p, q] = jnp.concatenate(shares, axis=1).astype(BF16)
        gathered = [
            send(hid.at[layer, p, q], hid.at[layer, p, q], s3.at[layer, d - 1], r3.at[layer, d - 1], q_peer(d))
            for d in far_first(n)
        ]
        for copy in gathered:
            copy.wait_recv()
        groups = {
            d: send(hid.at[layer, p], hid.at[layer, p], s4.at[layer, d - 1], r4.at[layer, d - 1], p_peer(d))
            for d in far_first(n)
        }
        loads[5 + layer].wait()
        from_peer[layer][2].wait_recv()
        for d in [0] + far_first(n)[::-1]:
            if d:
                groups[d].wait_recv()
            sender = lax.rem(p + n - d, n)
            units = hid[layer, sender].reshape(group, 2 * width)
            weights = down[layer].reshape(2 * width, -1)
            product = jnp.dot(units, weights, preferred_element_type=F32)
            part[layer, pl.ds(sender * (nz // n), nz // n)] = product.reshape(nz // n, zrows, -1)
        down_parts = []
        for d in far_first(nz):
            send3[layer, d - 1] = part[layer, lax.rem(z + d, nz)].astype(BF16)
            down_parts.append(send(
                send3.at[layer, d - 1], recv3.at[layer, d - 1], s5.at[layer, d - 1], r5.at[layer, d - 1], z_peer(d)
            ))
        branch = part[layer, z]
        for copy in down_parts:
            copy.wait_recv()
        for e in range(nz - 1):
            branch = branch + recv3[layer, e].astype(F32)
        new = (KEEP * stream[layer, z].astype(F32) + branch).astype(BF16)
        if layer + 1 < LAYERS:
            stream[layer + 1, z] = new
            rest = [
                send(stream.at[layer + 1, z], stream.at[layer + 1, z], s6.at[d - 1], r6.at[d - 1], z_peer(d))
                for d in far_first(nz)
            ]
            for copy in rest:
                copy.wait_recv()
        else:
            out[c * nz + z] = new
            rest = {
                d: send(out.at[c * nz + z], out.at[c * nz + z], s7.at[0, d - 1], r7.at[0, d - 1], z_peer(d))
                for d in far_first(nz)
            }
            passed = [send(out.at[c * nz + z], out.at[c * nz + z], s7.at[1, nz - 1], r7.at[1, nz - 1], other)]
            for d in far_first(nz)[::-1]:
                rest[d].wait_recv()
                at = c * nz + lax.rem(z + nz - d, nz)
                passed.append(send(out.at[at], out.at[at], s7.at[1, d - 1], r7.at[1, d - 1], other))
            for copy in passed:
                copy.wait_recv()
    for copy in pending:
        copy.wait_send()


def solution(mesh):
    zc = mesh.shape["cb"]
    n, nz = 4, zc // 2
    if mesh.shape["ra"] != n * n:
        n = 2
    torus = Mesh(mesh.devices.reshape(n, n, nz, 2), ("y", "x", "z", "c"))
    ra, cb = ("y", "x"), ("z", "c")

    def body(tokens, norm_gain, gate_weight, up_weight, down_weight):
        count, depth = tokens.shape
        width = gate_weight.shape[2]
        half = count // 2
        group, rows, zrows = half // n, half // (n * n), half // nz
        wide = 2 * width + 128
        dma = pltpu.SemaphoreType.DMA
        scratch = [
            pltpu.VMEM((LAYERS, nz, zrows, depth), BF16),
            pltpu.VMEM((LAYERS, depth), F32),
            pltpu.VMEM((LAYERS, 2, depth, width), BF16),
            pltpu.VMEM((LAYERS, 2, depth, width), BF16),
            pltpu.VMEM((LAYERS, 2, depth, 2 * width), BF16),
            pltpu.VMEM((LAYERS, 2, width, depth), BF16),
            pltpu.VMEM((LAYERS, 2, n - 1, group, wide), BF16),
            pltpu.VMEM((LAYERS, 2, n - 1, group, wide), BF16),
            pltpu.VMEM((LAYERS, 2, group, wide), F32),
            pltpu.VMEM((LAYERS, 2, n - 1, rows, wide), BF16),
            pltpu.VMEM((LAYERS, 2, n - 1, rows, wide), BF16),
            pltpu.VMEM((LAYERS, 2, rows, wide), F32),
            pltpu.VMEM((LAYERS, n, n, rows, 2 * width), BF16),
            pltpu.VMEM((LAYERS, nz, zrows, depth), F32),
            pltpu.VMEM((LAYERS, nz - 1, zrows, depth), BF16),
            pltpu.VMEM((LAYERS, nz - 1, zrows, depth), BF16),
            dma((7 + nz,)),
            dma((2, LAYERS, 3)),
            *[dma((LAYERS, 2, n - 1))] * 4,
            *[dma((LAYERS, n - 1))] * 4,
            *[dma((LAYERS, nz - 1))] * 2,
            *[dma((nz - 1,))] * 2,
            *[dma((2, nz))] * 2,
        ]
        result = pl.pallas_call(
            functools.partial(kernel, n, nz, depth * n * n),
            out_shape=jax.ShapeDtypeStruct((2 * nz, zrows, depth), BF16),
            in_specs=[pl.BlockSpec(memory_space=pl.ANY)] * 5,
            out_specs=pl.BlockSpec(memory_space=pltpu.VMEM),
            scratch_shapes=scratch,
            compiler_params=pltpu.CompilerParams(
                collective_id=0, has_side_effects=True, vmem_limit_bytes=60 * 1024 * 1024
            ),
        )(tokens, norm_gain, gate_weight, up_weight, down_weight)
        return result.reshape(count, depth)

    in_specs = (P(None, ra), P(None, ra), P(None, ra, cb), P(None, ra, cb), P(None, cb, ra))
    return jax.shard_map(body, mesh=torus, in_specs=in_specs, out_specs=P(None, ra), check_vma=False)
```

time: 291 us -> 100 us (0.34)
  blocking collectives: 126 us -> 0 us
  waiting for transfers between devices: 112 us -> 0 us
  Pallas kernels: 0 us -> 95.1 us
  starting transfers between devices: 14.3 us -> 0 us
  between operations: 13.6 us -> 0.01 us
  other arithmetic: 11.9 us -> 0 us
  matrix products: 6.18 us -> 0 us
    all_gather x2 -> x0, waiting for transfers between devices: 112 us -> none  [gathered_total(): blocks = lax.all_gather(array, axis)]
    psum x4 -> x0, blocking collectives: 95.4 us -> none  [over_axes(): return functools.reduce(lax.psum, axes, array)]
    pallas_call x0 -> x1, Pallas kernels: none -> 95.1 us  [body(): pl.pallas_call(functools.partial(kernel, n, nz, depth * n * n), out_shape...]
    all_to_all x2 -> x0, blocking collectives: 30.9 us -> none  [copy_for_each(): return lax.all_to_all(copies, axis, split_axis=0, concat_axis=0, tiled=True)]
    all_to_all x2 -> x0, starting transfers between devices: 14.2 us -> none  [sent_and_summed(): blocks = lax.all_to_all(in_blocks(array, dim, size), axis, 0, 0, tiled=True)]
    reduce_sum x6 -> x0, other arithmetic: 9.47 us -> none  [the longest x2 8.06 us: gathered_total(): return blocks.sum(axis=0)]
    dot_general x6 -> x0, matrix products: 6.18 us -> none  [the longest x2 2.52 us: body(): jnp.dot(hidden, down_weight[layer], preferred_element_type=jnp.float32)]
    unnamed x14 -> x5, local copies, waits for them, and re-layouts: 0.59 us -> 5.19 us
  transfers between devices with their start and end apart: 4 -> 0, of which waited for: 2 -> 0; matrix products, arithmetic and copies ran while one was open for 0% -> 0% of each run, Pallas kernels for 0% -> 0%
where the time goes in v1:
time: 100 us
  Pallas kernels  95.1 us (95%)
  local copies, waits for them, and re-layouts  5.19 us (5%)
    pallas_call x1, Pallas kernels, body(): pl.pallas_call(functools.partial(kernel, n, nz, depth * n * n), out_shape...  95.1 us
    unnamed x5, local copies, waits for them, and re-layouts  5.19 us

profile of v1, /device:TPU:1, one launch (start us, length us, event | category | flops | bytes accessed | tf_op | source)
XLA Modules:
  0.0 100.3 jit_solution(14526530179368714326)
XLA Ops:
  0.0 0.0 copy-start
  0.0 2.3 %copy.6.wg = bf16[2,256,704]{2,1,0:T(8,128)(2,1)} copy(bf16[2,256,704]{1,2,0:T(8,128)(2,1)} %param.7) | data formatting | bytes 1441792 | tf_op args[2]
  2.3 0.0 copy-done
  2.3 1.2 %copy.7.wu = bf16[2,256,704]{2,1,0:T(8,128)(2,1)} copy(bf16[2,256,704]{1,2,0:T(8,128)(2,1)S(1)} %copy-done) | data formatting | bytes 1441792 | tf_op args[3]
  3.5 95.1 %shard_map.55 = bf16[16,32,256]{2,1,0:T(8,128)(2,1)} custom-call(bf16[512,256]{1,0:T(8,128)(2,1)} %tok.1, f32[2,256]{1,0:T(2,128)} %gain.1, bf16[2,256,704]{2,1,0:T(8,128)(2,1)} %copy.6.wg, bf16[2,256,704]{2,1,0:T(8,128)(2,1)} %copy.7.wu, bf16[2,704,256]{2,1,0:T(8,128)(2,1)} %wd.1), custom_call_target="tpu_custom_call" | custom-call | tf_op jit(solution)/shard_map/pallas_call | solution.py:278
  98.6 1.7 %copy.9 = bf16[512,256]{1,0:T(8,128)(2,1)} copy(bf16[512,256]{1,0:T(8,128)(2,1)} %bitcast.1) | data formatting | bytes 524288
Async XLA Ops:
  0.0 2.3 %copy-start = (bf16[2,256,704]{1,2,0:T(8,128)(2,1)S(1)}, bf16[2,256,704]{1,2,0:T(8,128)(2,1)}, u32[]{:S(2)}) copy-start(bf16[2,256,704]{1,2,0:T(8,128)(2,1)} %param.8) | copy-start | bytes 2162692

commit v2 on v0

v2 whole, which is shorter than its diff:
```python
import functools

import jax
import jax.numpy as jnp
from jax import lax
from jax.experimental import pallas as pl
from jax.experimental.pallas import tpu as pltpu
from jax.sharding import Mesh
from jax.sharding import PartitionSpec as P

MESH = pl.DeviceIdType.MESH
LAYERS = 2
EPSILON = 1e-06
KEEP = 0.5
F32 = jnp.float32
BF16 = jnp.bfloat16
OVER_LAST = (((1,), (1,)), ((), ()))


def far_first(n):
    return sorted(range(1, n), key=lambda d: (-min(d, n - d), d))


def near_first(n):
    return far_first(n)[::-1]


def kernel(n, nz, features, tok, gain, wg, wu, wd, out, *scratch):
    (
        stream, gains, wcat, down, nbuf, squares, send2, recv2, own2, hid, part, send3, recv3,
        load_sem, gs, gr, ws, wr, ds, dr, ts, tr, s2, r2, s3, r3, s4, r4, s5, r5, s6, r6, s7, r7,
    ) = scratch
    y, x, z, c = (lax.axis_index(a) for a in ("y", "x", "z", "c"))
    _, _, _, zrows, depth = stream.shape
    half = nz * zrows
    group = half // n
    slices = nz // n
    pw = down.shape[2]
    wide = wcat.shape[2]
    halves = n // 2
    p = c * x + (1 - c) * y
    q = c * y + (1 - c) * x

    def p_peer(d):
        return {"y": lax.rem(y + (1 - c) * d, n), "x": lax.rem(x + c * d, n)}

    def q_peer(d):
        return {"y": lax.rem(y + c * d, n), "x": lax.rem(x + (1 - c) * d, n)}

    def z_peer(d):
        return {"z": lax.rem(z + d, nz)}

    other = {"c": 1 - c}
    pending = []

    def copy_to(src, dst, ss, rs, to):
        return pltpu.make_async_remote_copy(src, dst, ss, rs, device_id=to, device_id_type=MESH)

    def send(*where):
        copy = copy_to(*where)
        copy.start()
        pending.append(copy)
        return copy

    barrier = pltpu.get_barrier_semaphore()
    greeted = [p_peer(d) for d in range(1, n)] + [q_peer(d) for d in range(1, n)]
    greeted += [{**peer, "c": 1 - c} for peer in greeted]
    greeted += [z_peer(d) for d in range(1, nz)] + [other]
    for peer in greeted:
        pl.semaphore_signal(barrier, 1, device_id=peer, device_id_type=MESH)

    token_loads = [
        pltpu.make_async_copy(tok.at[pl.ds(c * half + k * zrows, zrows)], stream.at[0, 0, k], load_sem.at[k])
        for k in range(nz)
    ]
    token_loads.append(pltpu.make_async_copy(gain, gains.at[0], load_sem.at[nz]))
    down_loads = [
        [
            pltpu.make_async_copy(
                wd.at[layer, pl.ds(h * pw, pw)], down.at[layer, c * halves + h], load_sem.at[nz + 1 + layer * halves + h]
            )
            for h in range(halves)
        ]
        for layer in range(LAYERS)
    ]
    for copy in token_loads + down_loads[0] + down_loads[1]:
        copy.start()
    wcat[:, :, 2 * pw :, :] = jnp.zeros((LAYERS, n, wide - 2 * pw, depth), BF16)
    for copy in token_loads:
        copy.wait()
    pl.semaphore_wait(barrier, len(greeted))

    first = {0: {}}
    for d in far_first(n):
        first[d] = [
            send(gains.at[0], gains.at[d], gs.at[d - 1], gr.at[d - 1], p_peer(d)),
            send(stream.at[0, 0], stream.at[0, d], ts.at[d - 1], tr.at[d - 1], p_peer(d)),
        ]

    def deal_parts(layer, start):
        for t in range(2):
            a = x if t else y
            for h in range(halves):
                owner = c * halves + h
                d = lax.rem(owner - a + n, n)
                to = {"x" if t else "y": owner, "c": t}
                here = jnp.logical_and(c == t, owner == a)
                for k, w in enumerate((wg, wu)):
                    src = w.at[layer, pl.ds(h * pw, pw)]
                    dst = wcat.at[layer, d, pl.ds(k * pw, pw)]
                    sem = ws.at[layer, t, h, k]

                    @pl.when(jnp.logical_and(here, start))
                    def _():
                        pltpu.make_async_copy(src, dst, wr.at[layer, d, k]).start()

                    @pl.when(jnp.logical_not(here))
                    def _():
                        copy = copy_to(src, dst, sem, wr.at[layer, d, k], to)
                        if start:
                            copy.start()
                        else:
                            copy.wait_send()

    def wait_parts(layer):
        for d in range(n):
            for k in range(2):
                dst = wcat.at[layer, d, pl.ds(k * pw, pw)]
                pltpu.make_async_copy(wg.at[layer, pl.ds(0, pw)], dst, wr.at[layer, d, k]).wait()

    deal_parts(0, True)
    from_other = [
        [
            send(
                wd.at[layer, pl.ds(h * pw, pw)], down.at[layer, c * halves + h],
                ds.at[layer, h], dr.at[layer, h], other,
            )
            for h in range(halves)
        ]
        for layer in range(LAYERS)
    ]

    lane = lax.broadcasted_iota(jnp.int32, (1, 128), 1)

    def in_tile(high, low):
        return jnp.where(lane < 64, 0.0, jnp.where(lane < 96, high, low))

    def normalize(layer, at, slots):
        total = 0.0
        for d in range(n):
            tokens = stream[layer, d, at].astype(F32)
            nbuf[layer, at, :, d * depth : (d + 1) * depth] = (tokens * gains[d, layer : layer + 1]).astype(BF16)
            total = total + jnp.sum(tokens * tokens, axis=1, keepdims=True)
        squares[layer, at] = jnp.broadcast_to(total, (zrows, 128))

    arriving = None
    for layer in range(LAYERS):
        if layer == 0:
            for d in near_first(n):
                for copy in first[d]:
                    copy.wait_recv()
            for k in range(nz):
                normalize(layer, k, n)
        else:
            for e in [0] + near_first(nz):
                for d in near_first(n):
                    arriving[e][d].wait_recv()
                normalize(layer, lax.rem(z + nz - e, nz), n)
        wait_parts(layer)
        sums = {}
        for d in far_first(n) + [0]:
            to = pl.ds(lax.rem(q + d, n) * slices, slices)
            product = 0.0
            for e in range(n):
                normed = nbuf[layer, to, :, e * depth : (e + 1) * depth].reshape(group, depth)
                product = product + lax.dot_general(normed, wcat[layer, e], OVER_LAST, preferred_element_type=F32)
            total = squares[layer, to].reshape(group, 128)
            high = total.astype(BF16).astype(F32)
            last = product[:, wide - 128 :]
            if d == 0:
                own2[layer, :, : wide - 128] = product[:, : wide - 128]
                own2[layer, :, wide - 128 :] = last + in_tile(total, 0.0)
            else:
                send2[layer, d - 1, :, : wide - 128] = product[:, : wide - 128].astype(BF16)
                send2[layer, d - 1, :, wide - 128 :] = (last + in_tile(high, total - high)).astype(BF16)
                sums[d] = send(
                    send2.at[layer, d - 1], recv2.at[layer, d - 1], s2.at[layer, d - 1], r2.at[layer, d - 1], q_peer(d)
                )
        total = own2[layer]
        for d in near_first(n):
            sums[d].wait_recv()
            total = total + recv2[layer, d - 1].astype(F32)
        norm = total[:, wide - 64 : wide - 63] + total[:, wide - 32 : wide - 31]
        scale = lax.rsqrt(norm / features + EPSILON)
        gate = total[:, :pw] * scale
        up = total[:, pw : 2 * pw] * scale
        hid[layer, p, q] = (gate / (1.0 + jnp.exp(-gate)) * up).astype(BF16)
        across = {}
        pieces = {0: {}}

        def spread(e):
            at = hid.at[layer, p, lax.rem(q + n - e, n)]
            pieces[e] = {
                d: send(at, at, s4.at[layer, e, d - 1], r4.at[layer, e, d - 1], p_peer(d)) for d in far_first(n)
            }

        for d in far_first(n):
            at = hid.at[layer, p, q]
            across[d] = send(at, at, s3.at[layer, d - 1], r3.at[layer, d - 1], q_peer(d))
        spread(0)
        for d in near_first(n):
            across[d].wait_recv()
            spread(d)
        for copy in down_loads[layer]:
            copy.wait()
        for copy in from_other[layer]:
            copy.wait_recv()
        for e in [0] + near_first(n):
            for d in near_first(n):
                pieces[e][d].wait_recv()
            at = lax.rem(q + n - e, n)
            product = 0.0
            for k in range(n):
                product = product + jnp.dot(hid[layer, k, at], down[layer, k], preferred_element_type=F32)
            part[layer, pl.ds(at * slices, slices)] = product.reshape(slices, zrows, depth)
        down_parts = {}
        for d in far_first(nz):
            send3[layer, d - 1] = part[layer, lax.rem(z + d, nz)].astype(BF16)
            down_parts[d] = send(
                send3.at[layer, d - 1], recv3.at[layer, d - 1], s5.at[layer, d - 1], r5.at[layer, d - 1], z_peer(d)
            )
        if layer + 1 < LAYERS:
            deal_parts(layer + 1, True)
        branch = part[layer, z]
        for d in near_first(nz):
            down_parts[d].wait_recv()
            branch = branch + recv3[layer, d - 1].astype(F32)
        new = (KEEP * stream[layer, 0, z].astype(F32) + branch).astype(BF16)
        if layer + 1 < LAYERS:
            stream[layer + 1, 0, z] = new
            arriving = {}

            def pass_on(e):
                k = lax.rem(z + nz - e, nz)
                arriving[e] = {
                    d: send(
                        stream.at[layer + 1, 0, k], stream.at[layer + 1, d, k], s6.at[e, d], r6.at[e, d], p_peer(d)
                    )
                    for d in far_first(n)
                }

            at = stream.at[layer + 1, 0, z]
            along = {d: send(at, at, s6.at[d, 0], r6.at[d, 0], z_peer(d)) for d in far_first(nz)}
            pass_on(0)
            for e in near_first(nz):
                along[e].wait_recv()
                pass_on(e)
        else:
            mine = out.at[c * nz + z]
            out[c * nz + z] = new
            rest = {d: send(mine, mine, s7.at[0, d - 1], r7.at[0, d - 1], z_peer(d)) for d in far_first(nz)}
            passed = [send(mine, mine, s7.at[1, nz - 1], r7.at[1, nz - 1], other)]
            for d in near_first(nz):
                rest[d].wait_recv()
                at = out.at[c * nz + lax.rem(z + nz - d, nz)]
                passed.append(send(at, at, s7.at[1, d - 1], r7.at[1, d - 1], other))
            for copy in passed:
                copy.wait_recv()
    for copy in pending:
        copy.wait_send()
    for layer in range(LAYERS):
        deal_parts(layer, False)


def solution(mesh):
    nz = mesh.shape["cb"] // 2
    n = 4 if mesh.shape["ra"] == 16 else 2
    torus = Mesh(mesh.devices.reshape(n, n, nz, 2), ("y", "x", "z", "c"))
    ra, cb = ("y", "x"), ("z", "c")

    def body(tokens, norm_gain, gate_weight, up_weight, down_weight):
        count, depth = tokens.shape
        pw = gate_weight.shape[2] * 2 // n
        half = count // 2
        group, zrows = half // n, half // nz
        wide = pl.cdiv(2 * pw + 64, 128) * 128
        dma = pltpu.SemaphoreType.DMA
        scratch = [
            pltpu.VMEM((LAYERS, n, nz, zrows, depth), BF16),
            pltpu.VMEM((n, LAYERS, depth), F32),
            pltpu.VMEM((LAYERS, n, wide, depth), BF16),
            pltpu.VMEM((LAYERS, n, pw, depth), BF16),
            pltpu.VMEM((LAYERS, nz, zrows, n * depth), BF16),
            pltpu.VMEM((LAYERS, nz, zrows, 128), F32),
            pltpu.VMEM((LAYERS, n - 1, group, wide), BF16),
            pltpu.VMEM((LAYERS, n - 1, group, wide), BF16),
            pltpu.VMEM((LAYERS, group, wide), F32),
            pltpu.VMEM((LAYERS, n, n, group, pw), BF16),
            pltpu.VMEM((LAYERS, nz, zrows, depth), F32),
            pltpu.VMEM((LAYERS, nz - 1, zrows, depth), BF16),
            pltpu.VMEM((LAYERS, nz - 1, zrows, depth), BF16),
            dma((nz + 1 + LAYERS * (n // 2),)),
            *[dma((n - 1,))] * 2,
            dma((LAYERS, 2, n // 2, 2)),
            dma((LAYERS, n, 2)),
            *[dma((LAYERS, n // 2))] * 2,
            *[dma((n - 1,))] * 2,
            *[dma((LAYERS, n - 1))] * 4,
            *[dma((LAYERS, n, n - 1))] * 2,
            *[dma((LAYERS, nz - 1))] * 2,
            *[dma((nz, n))] * 2,
            *[dma((2, nz))] * 2,
        ]
        result = pl.pallas_call(
            functools.partial(kernel, n, nz, depth * n * n),
            out_shape=jax.ShapeDtypeStruct((2 * nz, zrows, depth), BF16),
            in_specs=[pl.BlockSpec(memory_space=pl.ANY)] * 5,
            out_specs=pl.BlockSpec(memory_space=pltpu.VMEM),
            scratch_shapes=scratch,
            compiler_params=pltpu.CompilerParams(
                collective_id=0, has_side_effects=True, vmem_limit_bytes=60 * 1024 * 1024
            ),
        )(tokens, norm_gain, jnp.swapaxes(gate_weight, 1, 2), jnp.swapaxes(up_weight, 1, 2), down_weight)
        return result.reshape(count, depth)

    in_specs = (P(None, ra), P(None, ra), P(None, ra, cb), P(None, ra, cb), P(None, cb, ra))
    return jax.shard_map(body, mesh=torus, in_specs=in_specs, out_specs=P(None, ra), check_vma=False)
```

time: 291 us -> 94.8 us (0.33)
  blocking collectives: 126 us -> 0 us
  waiting for transfers between devices: 112 us -> 0 us
  Pallas kernels: 0 us -> 92.9 us
  starting transfers between devices: 14.3 us -> 0 us
  between operations: 13.6 us -> 0.01 us
  other arithmetic: 11.9 us -> 0 us
  matrix products: 6.18 us -> 0 us
  local copies, waits for them, and re-layouts: 5.42 us -> 1.67 us
    all_gather x2 -> x0, waiting for transfers between devices: 112 us -> none  [gathered_total(): blocks = lax.all_gather(array, axis)]
    psum x4 -> x0, blocking collectives: 95.4 us -> none  [over_axes(): return functools.reduce(lax.psum, axes, array)]
    pallas_call x0 -> x1, Pallas kernels: none -> 92.9 us  [body(): pl.pallas_call(functools.partial(kernel, n, nz, depth * n * n), out_shape...]
    all_to_all x2 -> x0, blocking collectives: 30.9 us -> none  [copy_for_each(): return lax.all_to_all(copies, axis, split_axis=0, concat_axis=0, tiled=True)]
    all_to_all x2 -> x0, starting transfers between devices: 14.2 us -> none  [sent_and_summed(): blocks = lax.all_to_all(in_blocks(array, dim, size), axis, 0, 0, tiled=True)]
    reduce_sum x6 -> x0, other arithmetic: 9.47 us -> none  [the longest x2 8.06 us: gathered_total(): return blocks.sum(axis=0)]
    dot_general x6 -> x0, matrix products: 6.18 us -> none  [the longest x2 2.52 us: body(): jnp.dot(hidden, down_weight[layer], preferred_element_type=jnp.float32)]
    reshape x4 -> x0, local copies, waits for them, and re-layouts: 3.93 us -> none  [the longest x2 3.66 us: in_blocks(): array.reshape(*shape[:dim], size, shape[dim] // size, *shape[dim + 1:])]
  transfers between devices with their start and end apart: 4 -> 0, of which waited for: 2 -> 0; matrix products, arithmetic and copies ran while one was open for 0% -> 0% of each run, Pallas kernels for 0% -> 0%
where the time goes in v2:
time: 94.8 us; the launch traced here: 94.6 us
  Pallas kernels  92.9 us (98%)
  local copies, waits for them, and re-layouts  1.67 us (2%)
    pallas_call x1, Pallas kernels, body(): pl.pallas_call(functools.partial(kernel, n, nz, depth * n * n), out_shape...  92.9 us

profile of v2, /device:TPU:1, one launch (start us, length us, event | category | flops | bytes accessed | tf_op | source)
XLA Modules:
  0.0 94.6 jit_solution(15515184904527294966)
XLA Ops:
  0.0 92.9 %shard_map.55 = bf16[16,32,256]{2,1,0:T(8,128)(2,1)} custom-call(bf16[512,256]{1,0:T(8,128)(2,1)} %tok.1, f32[2,256]{1,0:T(2,128)} %gain.1, bf16[2,704,256]{2,1,0:T(8,128)(2,1)} %bitcast.4, bf16[2,704,256]{2,1,0:T(8,128)(2,1)} %bitcast.5, bf16[2,704,256]{2,1,0:T(8,128)(2,1)} %wd.1), custom_call_target="tpu_custom_call" | custom-call | tf_op jit(solution)/shard_map/pallas_call | solution.py:314
  92.9 1.7 %copy.7 = bf16[512,256]{1,0:T(8,128)(2,1)} copy(bf16[512,256]{1,0:T(8,128)(2,1)} %bitcast.3) | data formatting | bytes 524288

commit v3 on v0

v3 whole, which is shorter than its diff:
```python
import functools

import jax
import jax.numpy as jnp
from jax import lax
from jax.experimental import pallas as pl
from jax.experimental.pallas import tpu as pltpu
from jax.sharding import Mesh
from jax.sharding import PartitionSpec as P

MESH = pl.DeviceIdType.MESH
LAYERS = 2
EPSILON = 1e-06
KEEP = 0.5
F32 = jnp.float32
BF16 = jnp.bfloat16
OVER_LAST = (((1,), (1,)), ((), ()))


def far_first(n):
    return sorted(range(1, n), key=lambda d: (-min(d, n - d), d))


def near_first(n):
    return far_first(n)[::-1]


def kernel(n, nz, features, early, tok, gain, wg, wu, wd, out, *scratch):
    (
        tokens, stream, gains, w0, down0, w1, down1, nbuf, squares, own1, send1, recv1, own2, send2, recv2, hid0,
        own4, send4, recv4, hid1, part, send3, recv3,
        load_sem, gs, gr, ws, wr, ds, dr, s1, r1, s2, r2, s4, r4, sq, rq, sp, rp, sz, rz, ss, rs, so, ro,
    ) = scratch
    y, x, z, c = (lax.axis_index(a) for a in ("y", "x", "z", "c"))
    _, _, zrows, depth = stream.shape
    half = nz * zrows
    group = half // n
    rows = group // n
    slices = nz // n
    width = wg.shape[1]
    pw = down1.shape[1]
    wide = w1.shape[1]
    halves = n // 2
    cut = first_cut(width)
    p = c * x + (1 - c) * y
    q = c * y + (1 - c) * x

    def p_peer(d):
        return {"y": lax.rem(y + (1 - c) * d, n), "x": lax.rem(x + c * d, n)}

    def q_peer(d):
        return {"y": lax.rem(y + c * d, n), "x": lax.rem(x + (1 - c) * d, n)}

    def z_peer(d):
        return {"z": lax.rem(z + d, nz)}

    other = {"c": 1 - c}
    pending = []

    def copy_to(src, dst, ss, rs, to):
        return pltpu.make_async_remote_copy(src, dst, ss, rs, device_id=to, device_id_type=MESH)

    def send(*where):
        copy = copy_to(*where)
        copy.start()
        pending.append(copy)
        return copy

    barrier = pltpu.get_barrier_semaphore()
    greeted = [p_peer(d) for d in range(1, n)] + [q_peer(d) for d in range(1, n)]
    greeted += [{**peer, "c": 1 - c} for peer in greeted]
    greeted += [z_peer(d) for d in range(1, nz)] + [other]
    for peer in greeted:
        pl.semaphore_signal(barrier, 1, device_id=peer, device_id_type=MESH)

    loads = [
        pltpu.make_async_copy(gain, gains.at[0], load_sem.at[0]),
        pltpu.make_async_copy(tok, tokens, load_sem.at[1]),
        pltpu.make_async_copy(wg.at[0], w0.at[pl.ds(0, width)], load_sem.at[2]),
        pltpu.make_async_copy(wu.at[0], w0.at[pl.ds(width, width)], load_sem.at[3]),
    ]
    down_loads = [[pltpu.make_async_copy(wd.at[0], down0.at[0], load_sem.at[4])], [
        pltpu.make_async_copy(wd.at[1, pl.ds(h * pw, pw)], down1.at[c * halves + h], load_sem.at[5 + h])
        for h in range(halves)
    ]]
    for copy in loads + down_loads[0] + down_loads[1]:
        copy.start()
    w1[:, 2 * pw :, :] = jnp.zeros((n, wide - 2 * pw, depth), BF16)

    lane = lax.broadcasted_iota(jnp.int32, (1, 128), 1)
    edge = wide - 128

    def in_tile(high, low):
        return jnp.where(lane < 64, 0.0, jnp.where(lane < 96, high, low))

    def two_parts(total):
        high = total.astype(BF16).astype(F32)
        return in_tile(high, total - high)

    def all_squares(tile):
        return tile[:, 64:65] + tile[:, 96:97]

    for copy in loads:
        copy.wait()
    for at in range(2):
        mine = tokens[pl.ds((c if at == 0 else 1 - c) * half, half)].astype(F32)
        normed = (mine * gains[0, 0:1]).astype(BF16)
        product = lax.dot_general(normed, w0[...], OVER_LAST, preferred_element_type=F32)
        send1[at, :, :, 128:] = product.astype(BF16).reshape(n, group, 2 * width)
        if at == 0:
            own1[:, :, 128:] = product.reshape(n, group, 2 * width)
            total = jnp.sum(mine * mine, axis=1, keepdims=True)
            own1[:, :, :128] = in_tile(total, 0.0).reshape(n, group, 128)
            send1[0, :, :, :128] = two_parts(total).astype(BF16).reshape(n, group, 128)
    pl.semaphore_wait(barrier, len(greeted))

    spans = [[pl.ds(0, 128 + cut), pl.ds(128 + cut, 2 * width - cut)], [pl.ds(128, cut), pl.ds(128 + cut, 2 * width - cut)]]
    first = {}
    for piece in range(2):
        for d in far_first(n) + [0]:
            for at in range(2):
                if at == 0 and d == 0:
                    continue
                to = lax.rem((p, q)[at] + d, n)
                first[piece, at, d] = send(
                    send1.at[at, to, :, spans[at][piece]],
                    recv1.at[at, d, :, spans[at][piece]],
                    s1.at[piece, at, d],
                    r1.at[piece, at, d],
                    {**(p_peer, q_peer)[at](d), "c": (c, 1 - c)[at]},
                )
    for d in far_first(n):
        send(gains.at[0], gains.at[d], gs.at[d - 1], gr.at[d - 1], p_peer(d))
    from_other = [[send(wd.at[0], down0.at[1], ds.at[0], dr.at[0], other)], [
        send(wd.at[1, pl.ds(h * pw, pw)], down1.at[c * halves + h], ds.at[1 + h], dr.at[1 + h], other)
        for h in range(halves)
    ]]

    def deal_parts(kinds, start):
        for t in range(2):
            a = x if t else y
            for h in range(halves):
                owner = c * halves + h
                d = lax.rem(owner - a + n, n)
                to = {"x" if t else "y": owner, "c": t}
                here = jnp.logical_and(c == t, owner == a)
                for k in kinds:
                    src = (wg, wu)[k].at[1, pl.ds(h * pw, pw)]
                    dst = w1.at[d, pl.ds(k * pw, pw)]
                    sem = ws.at[t, h, k]

                    @pl.when(jnp.logical_and(here, start))
                    def _():
                        pltpu.make_async_copy(src, dst, wr.at[d, k]).start()

                    @pl.when(jnp.logical_not(here))
                    def _():
                        copy = copy_to(src, dst, sem, wr.at[d, k], to)
                        if start:
                            copy.start()
                        else:
                            copy.wait_send()

    second = {}
    bounds = [0, 128 + 2 * cut, 128 + 4 * width]
    for piece in range(2):
        for d in near_first(n) + [0]:
            for at in range(2):
                if at == 1 or d:
                    first[piece, at, d].wait_recv()
        for d in far_first(n) + [0]:
            at = pl.ds(pl.multiple_of(lax.rem(q + d, n) * rows, rows), rows)
            mine = own1[p, at, spans[0][piece]]
            for e in range(1, n):
                mine = mine + recv1[0, e, at, spans[0][piece]].astype(F32)
            theirs = recv1[1, 0, at, spans[1][piece]].astype(F32)
            for e in range(1, n):
                theirs = theirs + recv1[1, e, at, spans[1][piece]].astype(F32)
            total = [mine, theirs]
            if piece == 0:
                norm = all_squares(mine[:, :128])
                tile = two_parts(norm) if d else in_tile(norm, 0.0)
                total = [tile, mine[:, 128:], theirs]
            total = jnp.concatenate(total, axis=1)
            span = pl.ds(bounds[piece], bounds[piece + 1] - bounds[piece])
            if d == 0:
                own2[:, span] = total
            else:
                send2[d - 1, :, span] = total.astype(BF16)
                second[piece, d] = send(
                    send2.at[d - 1, :, span], recv2.at[d - 1, :, span],
                    s2.at[piece, d - 1], r2.at[piece, d - 1], q_peer(d),
                )
    sums = []
    for piece in range(2):
        span = pl.ds(bounds[piece], bounds[piece + 1] - bounds[piece])
        total = own2[:, span]
        for d in near_first(n):
            second[piece, d].wait_recv()
            total = total + recv2[d - 1, :, span].astype(F32)
        sums.append(total)
    scale = lax.rsqrt(all_squares(sums[0][:, :128]) / features + EPSILON)
    rest = 2 * width - cut
    shares = []
    for at in range(2):
        both = [sums[0][:, 128 + at * cut : 128 + (at + 1) * cut], sums[1][:, at * rest : (at + 1) * rest]]
        both = jnp.concatenate(both, axis=1) * scale
        shares.append(silu(both[:, :width]) * both[:, width:])
    hid0[p, q] = jnp.concatenate(shares, axis=1).astype(BF16)

    def gather(layer, hid, between):
        pieces = {}

        def spread(e):
            at = hid.at[p, lax.rem(q + n - e, n)]
            for d in far_first(n):
                pieces[e, d] = send(at, at, sp.at[layer, e, d - 1], rp.at[layer, e, d - 1], p_peer(d))

        at = hid.at[p, q]
        across = {d: send(at, at, sq.at[layer, d - 1], rq.at[layer, d - 1], q_peer(d)) for d in far_first(n)}
        spread(0)
        for d in near_first(n):
            across[d].wait_recv()
            spread(d)
        between()
        for copy in down_loads[layer]:
            copy.wait()
        for copy in from_other[layer]:
            copy.wait_recv()
        for e in [0] + near_first(n):
            for d in near_first(n):
                pieces[e, d].wait_recv()

    def sum_along_z(layer, product, before, between):
        part[layer] = product.reshape(nz, zrows, depth)
        copies = {}
        for d in far_first(nz):
            send3[layer, d - 1] = part[layer, lax.rem(z + d, nz)].astype(BF16)
            copies[d] = send(
                send3.at[layer, d - 1], recv3.at[layer, d - 1], sz.at[layer, d - 1], rz.at[layer, d - 1], z_peer(d)
            )
        between()
        branch = KEEP * before.astype(F32) + part[layer, z]
        for d in near_first(nz):
            copies[d].wait_recv()
            branch = branch + recv3[layer, d - 1].astype(F32)
        return branch.astype(BF16)

    def nothing():
        return None

    gather(0, hid0, (lambda: deal_parts((0, 1)[: early], True)) if early else nothing)
    product = jnp.dot(hid0[...].reshape(half, 2 * width), down0[...].reshape(2 * width, depth), preferred_element_type=F32)
    before = tokens[pl.ds(pl.multiple_of(c * half + z * zrows, zrows), zrows)]
    stream[0, z] = sum_along_z(0, product, before, lambda: deal_parts((0, 1)[early:], True))

    arriving = {}

    def pass_on(e):
        k = lax.rem(z + nz - e, nz)
        for d in far_first(n):
            arriving[e, d] = send(stream.at[0, k], stream.at[d, k], ss.at[e, d], rs.at[e, d], p_peer(d))

    def normalize(d, k):
        mine = stream[d, k].astype(F32)
        nbuf[k, :, d * depth : (d + 1) * depth] = (mine * gains[d, 1:2]).astype(BF16)
        mine = mine * mine
        parts = mine[:, :128]
        for b in range(1, depth // 128):
            parts = parts + mine[:, b * 128 : (b + 1) * 128]
        squares[d, k] = parts

    at = stream.at[0, z]
    along = {d: send(at, at, ss.at[d, 0], rs.at[d, 0], z_peer(d)) for d in far_first(nz)}
    pass_on(0)
    for e in near_first(nz):
        along[e].wait_recv()
        pass_on(e)
    for k in range(nz):
        normalize(0, k)
    for d in far_first(n):
        copy_to(gains.at[0], gains.at[d], gs.at[d - 1], gr.at[d - 1], p_peer(d)).wait_recv()
    for e in [0] + near_first(nz):
        for d in near_first(n):
            arriving[e, d].wait_recv()
            normalize(d, lax.rem(z + nz - e, nz))
    for d in range(n):
        for k in range(2):
            pltpu.make_async_copy(wg.at[1, pl.ds(0, pw)], w1.at[d, pl.ds(k * pw, pw)], wr.at[d, k]).wait()
    product = 0.0
    for e in range(n):
        normed = nbuf[:, :, e * depth : (e + 1) * depth].reshape(half, depth)
        product = product + lax.dot_general(normed, w1[e], OVER_LAST, preferred_element_type=F32)
    parts = squares[0]
    for d in range(1, n):
        parts = parts + squares[d]
    total = jnp.sum(parts.reshape(half, 128), axis=1, keepdims=True)
    own4[:, :, :edge] = product[:, :edge].reshape(n, group, edge)
    own4[:, :, edge:] = (product[:, edge:] + in_tile(total, 0.0)).reshape(n, group, 128)
    send4[:, :, :edge] = product[:, :edge].astype(BF16).reshape(n, group, edge)
    send4[:, :, edge:] = (product[:, edge:] + two_parts(total)).astype(BF16).reshape(n, group, 128)
    third = {
        d: send(send4.at[lax.rem(q + d, n)], recv4.at[d - 1], s4.at[d - 1], r4.at[d - 1], q_peer(d)) for d in far_first(n)
    }
    total = own4[q]
    for d in near_first(n):
        third[d].wait_recv()
        total = total + recv4[d - 1].astype(F32)
    both = total * lax.rsqrt(all_squares(total[:, edge:]) / features + EPSILON)
    hid1[p, q] = (silu(both[:, :pw]) * both[:, pw : 2 * pw]).astype(BF16)
    gather(1, hid1, nothing)
    product = 0.0
    for e in range(n):
        product = product + jnp.dot(hid1[e].reshape(half, pw), down1[e], preferred_element_type=F32)
    out[c * nz + z] = sum_along_z(1, product, stream[0, z], nothing)
    mine = out.at[c * nz + z]
    rest = {d: send(mine, mine, so.at[0, d - 1], ro.at[0, d - 1], z_peer(d)) for d in far_first(nz)}
    passed = [send(mine, mine, so.at[1, nz - 1], ro.at[1, nz - 1], other)]
    for d in near_first(nz):
        rest[d].wait_recv()
        at = out.at[c * nz + lax.rem(z + nz - d, nz)]
        passed.append(send(at, at, so.at[1, d - 1], ro.at[1, d - 1], other))
    for copy in passed:
        copy.wait_recv()
    for copy in pending:
        copy.wait_send()
    deal_parts((0, 1), False)


def first_cut(width):
    return pl.cdiv(2 * width, 256) * 128


def silu(v):
    return v / (1.0 + jnp.exp(-v))


EARLY = 0


def solution(mesh):
    nz = mesh.shape["cb"] // 2
    n = 4 if mesh.shape["ra"] == 16 else 2
    torus = Mesh(mesh.devices.reshape(n, n, nz, 2), ("y", "x", "z", "c"))
    ra, cb = ("y", "x"), ("z", "c")

    def body(tokens, norm_gain, gate_weight, up_weight, down_weight):
        count, depth = tokens.shape
        width = gate_weight.shape[2]
        pw = width * 2 // n
        half = count // 2
        group, zrows = half // n, half // nz
        wide = pl.cdiv(2 * pw + 64, 128) * 128
        dma = pltpu.SemaphoreType.DMA
        rows = group // n
        cols = 128 + 2 * width
        scratch = [
            pltpu.VMEM((count, depth), BF16),
            pltpu.VMEM((n, nz, zrows, depth), BF16),
            pltpu.VMEM((n, LAYERS, depth), F32),
            pltpu.VMEM((2 * width, depth), BF16),
            pltpu.VMEM((2, width, depth), BF16),
            pltpu.VMEM((n, wide, depth), BF16),
            pltpu.VMEM((n, pw, depth), BF16),
            pltpu.VMEM((nz, zrows, n * depth), BF16),
            pltpu.VMEM((n, nz, zrows, 128), F32),
            pltpu.VMEM((n, group, cols), F32),
            pltpu.VMEM((2, n, group, cols), BF16),
            pltpu.VMEM((2, n, group, cols), BF16),
            pltpu.VMEM((rows, 2 * cols - 128), F32),
            *[pltpu.VMEM((n - 1, rows, 2 * cols - 128), BF16)] * 2,
            pltpu.VMEM((n, n, rows, 2 * width), BF16),
            pltpu.VMEM((n, group, wide), F32),
            pltpu.VMEM((n, group, wide), BF16),
            pltpu.VMEM((n - 1, group, wide), BF16),
            pltpu.VMEM((n, n, group, pw), BF16),
            pltpu.VMEM((LAYERS, nz, zrows, depth), F32),
            *[pltpu.VMEM((LAYERS, nz - 1, zrows, depth), BF16)] * 2,
            dma((5 + n // 2,)),
            *[dma((n - 1,))] * 2,
            dma((2, n // 2, 2)),
            dma((n, 2)),
            *[dma((1 + n // 2,))] * 2,
            *[dma((2, 2, n))] * 2,
            *[dma((2, n - 1))] * 2,
            *[dma((n - 1,))] * 2,
            *[dma((LAYERS, n - 1))] * 2,
            *[dma((LAYERS, n, n - 1))] * 2,
            *[dma((LAYERS, nz - 1))] * 2,
            *[dma((nz, n))] * 2,
            *[dma((2, nz))] * 2,
        ]
        result = pl.pallas_call(
            functools.partial(kernel, n, nz, depth * n * n, EARLY),
            out_shape=jax.ShapeDtypeStruct((2 * nz, zrows, depth), BF16),
            in_specs=[pl.BlockSpec(memory_space=pl.ANY)] * 5,
            out_specs=pl.BlockSpec(memory_space=pltpu.VMEM),
            scratch_shapes=scratch,
            compiler_params=pltpu.CompilerParams(
                collective_id=0, has_side_effects=True, vmem_limit_bytes=60 * 1024 * 1024
            ),
        )(tokens, norm_gain, jnp.swapaxes(gate_weight, 1, 2), jnp.swapaxes(up_weight, 1, 2), down_weight)
        return result.reshape(count, depth)

    in_specs = (P(None, ra), P(None, ra), P(None, ra, cb), P(None, ra, cb), P(None, cb, ra))
    return jax.shard_map(body, mesh=torus, in_specs=in_specs, out_specs=P(None, ra), check_vma=False)
```

time: 291 us -> 87.4 us (0.30)
  blocking collectives: 126 us -> 0 us
  waiting for transfers between devices: 112 us -> 0 us
  Pallas kernels: 0 us -> 85.6 us
  starting transfers between devices: 14.3 us -> 0 us
  between operations: 13.6 us -> 0.01 us
  other arithmetic: 11.9 us -> 0 us
  matrix products: 6.18 us -> 0 us
  local copies, waits for them, and re-layouts: 5.42 us -> 1.67 us
    all_gather x2 -> x0, waiting for transfers between devices: 112 us -> none  [gathered_total(): blocks = lax.all_gather(array, axis)]
    psum x4 -> x0, blocking collectives: 95.4 us -> none  [over_axes(): return functools.reduce(lax.psum, axes, array)]
    pallas_call x0 -> x1, Pallas kernels: none -> 85.6 us  [body(): pl.pallas_call(functools.partial(kernel, n, nz, depth * n * n, EARLY), ou...]
    all_to_all x2 -> x0, blocking collectives: 30.9 us -> none  [copy_for_each(): return lax.all_to_all(copies, axis, split_axis=0, concat_axis=0, tiled=True)]
    all_to_all x2 -> x0, starting transfers between devices: 14.2 us -> none  [sent_and_summed(): blocks = lax.all_to_all(in_blocks(array, dim, size), axis, 0, 0, tiled=True)]
    reduce_sum x6 -> x0, other arithmetic: 9.47 us -> none  [the longest x2 8.06 us: gathered_total(): return blocks.sum(axis=0)]
    dot_general x6 -> x0, matrix products: 6.18 us -> none  [the longest x2 2.52 us: body(): jnp.dot(hidden, down_weight[layer], preferred_element_type=jnp.float32)]
    reshape x4 -> x0, local copies, waits for them, and re-layouts: 3.93 us -> none  [the longest x2 3.66 us: in_blocks(): array.reshape(*shape[:dim], size, shape[dim] // size, *shape[dim + 1:])]
  transfers between devices with their start and end apart: 4 -> 0, of which waited for: 2 -> 0; matrix products, arithmetic and copies ran while one was open for 0% -> 0% of each run, Pallas kernels for 0% -> 0%
where the time goes in v3:
time: 87.4 us; the launch traced here: 87.2 us
  Pallas kernels  85.6 us (98%)
  local copies, waits for them, and re-layouts  1.67 us (2%)
    pallas_call x1, Pallas kernels, body(): pl.pallas_call(functools.partial(kernel, n, nz, depth * n * n, EARLY), ou...  85.6 us

profile of v3, /device:TPU:1, one launch (start us, length us, event | category | flops | bytes accessed | tf_op | source)
XLA Modules:
  0.0 87.2 jit_solution(7441702091000093608)
XLA Ops:
  0.0 85.6 %shard_map.55 = bf16[16,32,256]{2,1,0:T(8,128)(2,1)} custom-call(bf16[512,256]{1,0:T(8,128)(2,1)} %tok.1, f32[2,256]{1,0:T(2,128)} %gain.1, bf16[2,704,256]{2,1,0:T(8,128)(2,1)} %bitcast.4, bf16[2,704,256]{2,1,0:T(8,128)(2,1)} %bitcast.5, bf16[2,704,256]{2,1,0:T(8,128)(2,1)} %wd.1), custom_call_target="tpu_custom_call" | custom-call | tf_op jit(solution)/shard_map/pallas_call | solution.py:393
  85.6 1.7 %copy.7 = bf16[512,256]{1,0:T(8,128)(2,1)} copy(bf16[512,256]{1,0:T(8,128)(2,1)} %bitcast.3) | data formatting | bytes 524288

commit v4 on v3

--- a/solution.py
+++ b/solution.py
@@ -25,11 +25,11 @@
     return far_first(n)[::-1]
 
 
-def kernel(n, nz, features, early, tok, gain, wg, wu, wd, out, *scratch):
+def kernel(n, nz, features, tok, gain, wg, wu, wd, out, *scratch):
     (
         tokens, stream, gains, w0, down0, w1, down1, nbuf, squares, own1, send1, recv1, own2, send2, recv2, hid0,
-        own4, send4, recv4, hid1, part, send3, recv3,
-        load_sem, gs, gr, ws, wr, ds, dr, s1, r1, s2, r2, s4, r4, sq, rq, sp, rp, sz, rz, ss, rs, so, ro,
+        own4, send4, recv4, hid1, part, send3, recv3, fresh,
+        staged, load_sem, gs, gr, ws, wr, ds, dr, s1, r1, s2, r2, s4, r4, sq, rq, sp, rp, sz, rz, ss, rs, so, ro,
     ) = scratch
     y, x, z, c = (lax.axis_index(a) for a in ("y", "x", "z", "c"))
     _, _, zrows, depth = stream.shape
@@ -69,7 +69,7 @@
     barrier = pltpu.get_barrier_semaphore()
     greeted = [p_peer(d) for d in range(1, n)] + [q_peer(d) for d in range(1, n)]
     greeted += [{**peer, "c": 1 - c} for peer in greeted]
-    greeted += [z_peer(d) for d in range(1, nz)] + [other]
+    greeted += [z_peer(d) for d in range(1, nz)] + [{**z_peer(d), **other} for d in range(nz)]
     for peer in greeted:
         pl.semaphore_signal(barrier, 1, device_id=peer, device_id_type=MESH)
 
@@ -83,7 +83,10 @@
         pltpu.make_async_copy(wd.at[1, pl.ds(h * pw, pw)], down1.at[c * halves + h], load_sem.at[5 + h])
         for h in range(halves)
     ]]
-    for copy in loads + down_loads[0] + down_loads[1]:
+    part_loads = [
+        pltpu.make_async_copy(w.at[1], staged.at[k], load_sem.at[5 + halves + k]) for k, w in enumerate((wg, wu))
+    ]
+    for copy in loads + down_loads[0] + down_loads[1] + part_loads:
         copy.start()
     w1[:, 2 * pw :, :] = jnp.zeros((n, wide - 2 * pw, depth), BF16)
 
@@ -112,6 +115,8 @@
             total = jnp.sum(mine * mine, axis=1, keepdims=True)
             own1[:, :, :128] = in_tile(total, 0.0).reshape(n, group, 128)
             send1[0, :, :, :128] = two_parts(total).astype(BF16).reshape(n, group, 128)
+    for copy in part_loads:
+        copy.wait()
     pl.semaphore_wait(barrier, len(greeted))
 
     spans = [[pl.ds(0, 128 + cut), pl.ds(128 + cut, 2 * width - cut)], [pl.ds(128, cut), pl.ds(128 + cut, 2 * width - cut)]]
@@ -136,7 +141,7 @@
         for h in range(halves)
     ]]
 
-    def deal_parts(kinds, start):
+    def deal_parts(point, start=True):
         for t in range(2):
             a = x if t else y
             for h in range(halves):
@@ -144,14 +149,16 @@
                 d = lax.rem(owner - a + n, n)
                 to = {"x" if t else "y": owner, "c": t}
                 here = jnp.logical_and(c == t, owner == a)
-                for k in kinds:
-                    src = (wg, wu)[k].at[1, pl.ds(h * pw, pw)]
+                for k in range(2):
+                    if start and DEAL[2 * k + h % 2] != point:
+                        continue
+                    src = staged.at[k, pl.ds(h * pw, pw)]
                     dst = w1.at[d, pl.ds(k * pw, pw)]
                     sem = ws.at[t, h, k]
 
                     @pl.when(jnp.logical_and(here, start))
                     def _():
-                        pltpu.make_async_copy(src, dst, wr.at[d, k]).start()
+                        pltpu.make_async_copy((wg, wu)[k].at[1, pl.ds(h * pw, pw)], dst, wr.at[d, k]).start()
 
                     @pl.when(jnp.logical_not(here))
                     def _():
@@ -191,6 +198,7 @@
                     send2.at[d - 1, :, span], recv2.at[d - 1, :, span],
                     s2.at[piece, d - 1], r2.at[piece, d - 1], q_peer(d),
                 )
+    deal_parts("r")
     sums = []
     for piece in range(2):
         span = pl.ds(bounds[piece], bounds[piece + 1] - bounds[piece])
@@ -208,7 +216,7 @@
         shares.append(silu(both[:, :width]) * both[:, width:])
     hid0[p, q] = jnp.concatenate(shares, axis=1).astype(BF16)
 
-    def gather(layer, hid, between):
+    def gather(layer, hid, between, after):
         pieces = {}
 
         def spread(e):
@@ -219,10 +227,11 @@
         at = hid.at[p, q]
         across = {d: send(at, at, sq.at[layer, d - 1], rq.at[layer, d - 1], q_peer(d)) for d in far_first(n)}
         spread(0)
+        between()
         for d in near_first(n):
             across[d].wait_recv()
             spread(d)
-        between()
+        after()
         for copy in down_loads[layer]:
             copy.wait()
         for copy in from_other[layer]:
@@ -249,10 +258,11 @@
     def nothing():
         return None
 
-    gather(0, hid0, (lambda: deal_parts((0, 1)[: early], True)) if early else nothing)
+    gather(0, hid0, lambda: deal_parts("q"), lambda: deal_parts("p"))
     product = jnp.dot(hid0[...].reshape(half, 2 * width), down0[...].reshape(2 * width, depth), preferred_element_type=F32)
     before = tokens[pl.ds(pl.multiple_of(c * half + z * zrows, zrows), zrows)]
-    stream[0, z] = sum_along_z(0, product, before, lambda: deal_parts((0, 1)[early:], True))
+    fresh[...] = sum_along_z(0, product, before, lambda: deal_parts("z"))
+    deal_parts("zz")
 
     arriving = {}
 
@@ -270,10 +280,10 @@
             parts = parts + mine[:, b * 128 : (b + 1) * 128]
         squares[d, k] = parts
 
-    at = stream.at[0, z]
-    along = {d: send(at, at, ss.at[d, 0], rs.at[d, 0], z_peer(d)) for d in far_first(nz)}
-    pass_on(0)
-    for e in near_first(nz):
+    along = {
+        d: send(fresh, stream.at[0, z], ss.at[d, 0], rs.at[d, 0], {**z_peer(d), **other}) for d in far_first(nz) + [0]
+    }
+    for e in [0] + near_first(nz):
         along[e].wait_recv()
         pass_on(e)
     for k in range(nz):
@@ -308,23 +318,23 @@
         total = total + recv4[d - 1].astype(F32)
     both = total * lax.rsqrt(all_squares(total[:, edge:]) / features + EPSILON)
     hid1[p, q] = (silu(both[:, :pw]) * both[:, pw : 2 * pw]).astype(BF16)
-    gather(1, hid1, nothing)
+    gather(1, hid1, nothing, nothing)
     product = 0.0
     for e in range(n):
         product = product + jnp.dot(hid1[e].reshape(half, pw), down1[e], preferred_element_type=F32)
-    out[c * nz + z] = sum_along_z(1, product, stream[0, z], nothing)
-    mine = out.at[c * nz + z]
+    out[(1 - c) * nz + z] = sum_along_z(1, product, stream[0, z], nothing)
+    mine = out.at[(1 - c) * nz + z]
     rest = {d: send(mine, mine, so.at[0, d - 1], ro.at[0, d - 1], z_peer(d)) for d in far_first(nz)}
     passed = [send(mine, mine, so.at[1, nz - 1], ro.at[1, nz - 1], other)]
     for d in near_first(nz):
         rest[d].wait_recv()
-        at = out.at[c * nz + lax.rem(z + nz - d, nz)]
+        at = out.at[(1 - c) * nz + lax.rem(z + nz - d, nz)]
         passed.append(send(at, at, so.at[1, d - 1], ro.at[1, d - 1], other))
     for copy in passed:
         copy.wait_recv()
     for copy in pending:
         copy.wait_send()
-    deal_parts((0, 1), False)
+    deal_parts(None, False)
 
 
 def first_cut(width):
@@ -335,7 +345,7 @@
     return v / (1.0 + jnp.exp(-v))
 
 
-EARLY = 0
+DEAL = ('p', 'p', 'z', 'z')
 
 
 def solution(mesh):
@@ -376,7 +386,9 @@
             pltpu.VMEM((n, n, group, pw), BF16),
             pltpu.VMEM((LAYERS, nz, zrows, depth), F32),
             *[pltpu.VMEM((LAYERS, nz - 1, zrows, depth), BF16)] * 2,
-            dma((5 + n // 2,)),
+            pltpu.VMEM((zrows, depth), BF16),
+            pltpu.VMEM((2, width, depth), BF16),
+            dma((7 + n // 2,)),
             *[dma((n - 1,))] * 2,
             dma((2, n // 2, 2)),
             dma((n, 2)),
@@ -391,7 +403,7 @@
             *[dma((2, nz))] * 2,
         ]
         result = pl.pallas_call(
-            functools.partial(kernel, n, nz, depth * n * n, EARLY),
+            functools.partial(kernel, n, nz, depth * n * n),
             out_shape=jax.ShapeDtypeStruct((2 * nz, zrows, depth), BF16),
             in_specs=[pl.BlockSpec(memory_space=pl.ANY)] * 5,
             out_specs=pl.BlockSpec(memory_space=pltpu.VMEM),

time: 87.4 us -> 85.8 us (0.982)
  Pallas kernels: 85.6 us -> 83.7 us
    pallas_call x1, Pallas kernels: 85.6 us -> 83.7 us  [body(): pl.pallas_call(functools.partial(kernel, n, nz, depth * n * n), out_shape...]
where the time goes in v4:
time: 85.8 us; the launch traced here: 85.4 us
  Pallas kernels  83.7 us (98%)
  local copies, waits for them, and re-layouts  1.67 us (2%)
    pallas_call x1, Pallas kernels, body(): pl.pallas_call(functools.partial(kernel, n, nz, depth * n * n), out_shape...  83.7 us

profile of v4, /device:TPU:1, one launch (start us, length us, event | category | flops | bytes accessed | tf_op | source)
XLA Modules:
  0.0 85.4 jit_solution(14471589773531763057)
XLA Ops:
  0.0 83.7 %shard_map.55 = bf16[16,32,256]{2,1,0:T(8,128)(2,1)} custom-call(bf16[512,256]{1,0:T(8,128)(2,1)} %tok.1, f32[2,256]{1,0:T(2,128)} %gain.1, bf16[2,704,256]{2,1,0:T(8,128)(2,1)} %bitcast.4, bf16[2,704,256]{2,1,0:T(8,128)(2,1)} %bitcast.5, bf16[2,704,256]{2,1,0:T(8,128)(2,1)} %wd.1), custom_call_target="tpu_custom_call" | custom-call | tf_op jit(solution)/shard_map/pallas_call | solution.py:405
  83.7 1.7 %copy.7 = bf16[512,256]{1,0:T(8,128)(2,1)} copy(bf16[512,256]{1,0:T(8,128)(2,1)} %bitcast.3) | data formatting | bytes 524288

commit v5 on v4

--- a/solution.py
+++ b/solution.py
@@ -32,11 +32,12 @@
         staged, load_sem, gs, gr, ws, wr, ds, dr, s1, r1, s2, r2, s4, r4, sq, rq, sp, rp, sz, rz, ss, rs, so, ro,
     ) = scratch
     y, x, z, c = (lax.axis_index(a) for a in ("y", "x", "z", "c"))
-    _, _, zrows, depth = stream.shape
-    half = nz * zrows
+    _, _, _, zrows, depth = stream.shape
+    chunk = nz * zrows
+    half = CHUNKS * chunk
     group = half // n
     rows = group // n
-    slices = nz // n
+    share = chunk // n
     width = wg.shape[1]
     pw = down1.shape[1]
     wide = w1.shape[1]
@@ -216,122 +217,153 @@
         shares.append(silu(both[:, :width]) * both[:, width:])
     hid0[p, q] = jnp.concatenate(shares, axis=1).astype(BF16)
 
-    def gather(layer, hid, between, after):
+    def gather(hid, semaphores, layer, between, after):
+        sq, rq, sp, rp = semaphores
         pieces = {}
 
         def spread(e):
             at = hid.at[p, lax.rem(q + n - e, n)]
             for d in far_first(n):
-                pieces[e, d] = send(at, at, sp.at[layer, e, d - 1], rp.at[layer, e, d - 1], p_peer(d))
+                pieces[e, d] = send(at, at, sp.at[e, d - 1], rp.at[e, d - 1], p_peer(d))
 
         at = hid.at[p, q]
-        across = {d: send(at, at, sq.at[layer, d - 1], rq.at[layer, d - 1], q_peer(d)) for d in far_first(n)}
+        across = {d: send(at, at, sq.at[d - 1], rq.at[d - 1], q_peer(d)) for d in far_first(n)}
         spread(0)
         between()
         for d in near_first(n):
+            yield
             across[d].wait_recv()
             spread(d)
         after()
+        yield
+        for e in [0] + near_first(n):
+            for d in near_first(n):
+                pieces[e, d].wait_recv()
+
+    def send_along_z(layer, k, product):
+        part[layer, k] = product.reshape(nz, zrows, depth)
+        copies = {}
+        for d in far_first(nz):
+            at = (layer, k, d - 1)
+            send3[at] = part[layer, k, lax.rem(z + d, nz)].astype(BF16)
+            copies[d] = send(send3.at[at], recv3.at[at], sz.at[at], rz.at[at], z_peer(d))
+        return copies
+
+    def sum_along_z(layer, k, copies, before):
+        branch = KEEP * before.astype(F32) + part[layer, k, z]
+        for d in near_first(nz):
+            copies[d].wait_recv()
+            branch = branch + recv3[layer, k, d - 1].astype(F32)
+        return branch.astype(BF16)
+
+    def nothing():
+        return None
+
+    def wait_down(layer):
         for copy in down_loads[layer]:
             copy.wait()
         for copy in from_other[layer]:
             copy.wait_recv()
-        for e in [0] + near_first(n):
-            for d in near_first(n):
-                pieces[e, d].wait_recv()
-
-    def sum_along_z(layer, product, before, between):
-        part[layer] = product.reshape(nz, zrows, depth)
-        copies = {}
-        for d in far_first(nz):
-            send3[layer, d - 1] = part[layer, lax.rem(z + d, nz)].astype(BF16)
-            copies[d] = send(
-                send3.at[layer, d - 1], recv3.at[layer, d - 1], sz.at[layer, d - 1], rz.at[layer, d - 1], z_peer(d)
-            )
-        between()
-        branch = KEEP * before.astype(F32) + part[layer, z]
-        for d in near_first(nz):
-            copies[d].wait_recv()
-            branch = branch + recv3[layer, d - 1].astype(F32)
-        return branch.astype(BF16)
-
-    def nothing():
-        return None
-
-    gather(0, hid0, lambda: deal_parts("q"), lambda: deal_parts("p"))
-    product = jnp.dot(hid0[...].reshape(half, 2 * width), down0[...].reshape(2 * width, depth), preferred_element_type=F32)
-    before = tokens[pl.ds(pl.multiple_of(c * half + z * zrows, zrows), zrows)]
-    fresh[...] = sum_along_z(0, product, before, lambda: deal_parts("z"))
-    deal_parts("zz")
-
-    arriving = {}
-
-    def pass_on(e):
-        k = lax.rem(z + nz - e, nz)
-        for d in far_first(n):
-            arriving[e, d] = send(stream.at[0, k], stream.at[d, k], ss.at[e, d], rs.at[e, d], p_peer(d))
-
-    def normalize(d, k):
-        mine = stream[d, k].astype(F32)
-        nbuf[k, :, d * depth : (d + 1) * depth] = (mine * gains[d, 1:2]).astype(BF16)
+
+    semaphores = [tuple(s.at[k] for s in (sq, rq, sp, rp)) for k in range(1 + CHUNKS)]
+    for _ in gather(hid0, semaphores[0], 0, nothing, lambda: deal_parts("p")):
+        pass
+    wait_down(0)
+
+    def normalize(g, d, k):
+        mine = stream[g, d, k].astype(F32)
+        nbuf[g, k, :, d * depth : (d + 1) * depth] = (mine * gains[d, 1:2]).astype(BF16)
         mine = mine * mine
         parts = mine[:, :128]
         for b in range(1, depth // 128):
             parts = parts + mine[:, b * 128 : (b + 1) * 128]
-        squares[d, k] = parts
-
-    along = {
-        d: send(fresh, stream.at[0, z], ss.at[d, 0], rs.at[d, 0], {**z_peer(d), **other}) for d in far_first(nz) + [0]
-    }
-    for e in [0] + near_first(nz):
-        along[e].wait_recv()
-        pass_on(e)
-    for k in range(nz):
-        normalize(0, k)
-    for d in far_first(n):
-        copy_to(gains.at[0], gains.at[d], gs.at[d - 1], gr.at[d - 1], p_peer(d)).wait_recv()
-    for e in [0] + near_first(nz):
+        squares[g, d, k] = parts
+
+    def finish(g):
+        lines = n // CHUNKS
+        units = hid0[g * lines : (g + 1) * lines].reshape(chunk, 2 * width)
+        product = jnp.dot(units, down0[...].reshape(2 * width, depth), preferred_element_type=F32)
+        copies = send_along_z(0, g, product)
+        yield
+        before = tokens[pl.ds(pl.multiple_of(c * half + g * chunk + z * zrows, zrows), zrows)]
+        fresh[g] = sum_along_z(0, g, copies, before)
+        along = {
+            d: send(fresh.at[g], stream.at[g, 0, z], ss.at[g, d, 0], rs.at[g, d, 0], {**z_peer(d), **other})
+            for d in far_first(nz) + [0]
+        }
+        arriving = {}
+        for e in [0] + near_first(nz):
+            yield
+            along[e].wait_recv()
+            k = lax.rem(z + nz - e, nz)
+            for d in far_first(n):
+                arriving[e, d] = send(stream.at[g, 0, k], stream.at[g, d, k], ss.at[g, e, d], rs.at[g, e, d], p_peer(d))
+        for k in range(nz):
+            normalize(g, 0, k)
+        if g == 0:
+            for d in far_first(n):
+                copy_to(gains.at[0], gains.at[d], gs.at[d - 1], gr.at[d - 1], p_peer(d)).wait_recv()
+        yield
+        for e in [0] + near_first(nz):
+            for d in near_first(n):
+                arriving[e, d].wait_recv()
+                normalize(g, d, lax.rem(z + nz - e, nz))
+        if g == 0:
+            for d in range(n):
+                for k in range(2):
+                    pltpu.make_async_copy(wg.at[1, pl.ds(0, pw)], w1.at[d, pl.ds(k * pw, pw)], wr.at[d, k]).wait()
+        product = 0.0
+        for e in range(n):
+            normed = nbuf[g, :, :, e * depth : (e + 1) * depth].reshape(chunk, depth)
+            product = product + lax.dot_general(normed, w1[e], OVER_LAST, preferred_element_type=F32)
+        parts = squares[g, 0]
+        for d in range(1, n):
+            parts = parts + squares[g, d]
+        total = jnp.sum(parts.reshape(chunk, 128), axis=1, keepdims=True)
+        own4[g, :, :, :edge] = product[:, :edge].reshape(n, share, edge)
+        own4[g, :, :, edge:] = (product[:, edge:] + in_tile(total, 0.0)).reshape(n, share, 128)
+        send4[g, :, :, :edge] = product[:, :edge].astype(BF16).reshape(n, share, edge)
+        send4[g, :, :, edge:] = (product[:, edge:] + two_parts(total)).astype(BF16).reshape(n, share, 128)
+        third = {
+            d: send(send4.at[g, lax.rem(q + d, n)], recv4.at[g, d - 1], s4.at[g, d - 1], r4.at[g, d - 1], q_peer(d))
+            for d in far_first(n)
+        }
+        yield
+        total = own4[g, q]
         for d in near_first(n):
-            arriving[e, d].wait_recv()
-            normalize(d, lax.rem(z + nz - e, nz))
-    for d in range(n):
-        for k in range(2):
-            pltpu.make_async_copy(wg.at[1, pl.ds(0, pw)], w1.at[d, pl.ds(k * pw, pw)], wr.at[d, k]).wait()
-    product = 0.0
-    for e in range(n):
-        normed = nbuf[:, :, e * depth : (e + 1) * depth].reshape(half, depth)
-        product = product + lax.dot_general(normed, w1[e], OVER_LAST, preferred_element_type=F32)
-    parts = squares[0]
-    for d in range(1, n):
-        parts = parts + squares[d]
-    total = jnp.sum(parts.reshape(half, 128), axis=1, keepdims=True)
-    own4[:, :, :edge] = product[:, :edge].reshape(n, group, edge)
-    own4[:, :, edge:] = (product[:, edge:] + in_tile(total, 0.0)).reshape(n, group, 128)
-    send4[:, :, :edge] = product[:, :edge].astype(BF16).reshape(n, group, edge)
-    send4[:, :, edge:] = (product[:, edge:] + two_parts(total)).astype(BF16).reshape(n, group, 128)
-    third = {
-        d: send(send4.at[lax.rem(q + d, n)], recv4.at[d - 1], s4.at[d - 1], r4.at[d - 1], q_peer(d)) for d in far_first(n)
-    }
-    total = own4[q]
-    for d in near_first(n):
-        third[d].wait_recv()
-        total = total + recv4[d - 1].astype(F32)
-    both = total * lax.rsqrt(all_squares(total[:, edge:]) / features + EPSILON)
-    hid1[p, q] = (silu(both[:, :pw]) * both[:, pw : 2 * pw]).astype(BF16)
-    gather(1, hid1, nothing, nothing)
-    product = 0.0
-    for e in range(n):
-        product = product + jnp.dot(hid1[e].reshape(half, pw), down1[e], preferred_element_type=F32)
-    out[(1 - c) * nz + z] = sum_along_z(1, product, stream[0, z], nothing)
-    mine = out.at[(1 - c) * nz + z]
-    rest = {d: send(mine, mine, so.at[0, d - 1], ro.at[0, d - 1], z_peer(d)) for d in far_first(nz)}
-    passed = [send(mine, mine, so.at[1, nz - 1], ro.at[1, nz - 1], other)]
-    for d in near_first(nz):
-        rest[d].wait_recv()
-        at = out.at[(1 - c) * nz + lax.rem(z + nz - d, nz)]
-        passed.append(send(at, at, so.at[1, d - 1], ro.at[1, d - 1], other))
-    for copy in passed:
-        copy.wait_recv()
+            third[d].wait_recv()
+            total = total + recv4[g, d - 1].astype(F32)
+        both = total * lax.rsqrt(all_squares(total[:, edge:]) / features + EPSILON)
+        hid1[g, p, q] = (silu(both[:, :pw]) * both[:, pw : 2 * pw]).astype(BF16)
+        yield from gather(hid1.at[g], semaphores[1 + g], 1, nothing, nothing)
+        if g == 0:
+            wait_down(1)
+        product = 0.0
+        for e in range(n):
+            product = product + jnp.dot(hid1[g, e].reshape(chunk, pw), down1[e], preferred_element_type=F32)
+        copies = send_along_z(1, g, product)
+        yield
+        mine = out.at[1 - c, g, z]
+        out[1 - c, g, z] = sum_along_z(1, g, copies, stream[g, 0, z])
+        rest = {d: send(mine, mine, so.at[g, 0, d - 1], ro.at[g, 0, d - 1], z_peer(d)) for d in far_first(nz)}
+        passed = [send(mine, mine, so.at[g, 1, nz - 1], ro.at[g, 1, nz - 1], other)]
+        for d in near_first(nz):
+            yield
+            rest[d].wait_recv()
+            at = out.at[1 - c, g, lax.rem(z + nz - d, nz)]
+            passed.append(send(at, at, so.at[g, 1, d - 1], ro.at[g, 1, d - 1], other))
+        yield
+        for copy in passed:
+            copy.wait_recv()
+
+    chunks = [finish(g) for g in range(CHUNKS)]
+    for steps in chunks:
+        next(steps)
+    deal_parts("z")
+    while chunks:
+        for steps in list(chunks):
+            if next(steps, chunks) is chunks:
+                chunks.remove(steps)
     for copy in pending:
         copy.wait_send()
     deal_parts(None, False)
@@ -345,6 +377,7 @@
     return v / (1.0 + jnp.exp(-v))
 
 
+CHUNKS = 2
 DEAL = ('p', 'p', 'z', 'z')
 
 
@@ -359,34 +392,35 @@
         width = gate_weight.shape[2]
         pw = width * 2 // n
         half = count // 2
-        group, zrows = half // n, half // nz
+        group, zrows = half // n, half // nz // CHUNKS
+        share = group // CHUNKS
         wide = pl.cdiv(2 * pw + 64, 128) * 128
         dma = pltpu.SemaphoreType.DMA
         rows = group // n
         cols = 128 + 2 * width
         scratch = [
             pltpu.VMEM((count, depth), BF16),
-            pltpu.VMEM((n, nz, zrows, depth), BF16),
+            pltpu.VMEM((CHUNKS, n, nz, zrows, depth), BF16),
             pltpu.VMEM((n, LAYERS, depth), F32),
             pltpu.VMEM((2 * width, depth), BF16),
             pltpu.VMEM((2, width, depth), BF16),
             pltpu.VMEM((n, wide, depth), BF16),
             pltpu.VMEM((n, pw, depth), BF16),
-            pltpu.VMEM((nz, zrows, n * depth), BF16),
-            pltpu.VMEM((n, nz, zrows, 128), F32),
+            pltpu.VMEM((CHUNKS, nz, zrows, n * depth), BF16),
+            pltpu.VMEM((CHUNKS, n, nz, zrows, 128), F32),
             pltpu.VMEM((n, group, cols), F32),
             pltpu.VMEM((2, n, group, cols), BF16),
             pltpu.VMEM((2, n, group, cols), BF16),
             pltpu.VMEM((rows, 2 * cols - 128), F32),
             *[pltpu.VMEM((n - 1, rows, 2 * cols - 128), BF16)] * 2,
             pltpu.VMEM((n, n, rows, 2 * width), BF16),
-            pltpu.VMEM((n, group, wide), F32),
-            pltpu.VMEM((n, group, wide), BF16),
-            pltpu.VMEM((n - 1, group, wide), BF16),
-            pltpu.VMEM((n, n, group, pw), BF16),
-            pltpu.VMEM((LAYERS, nz, zrows, depth), F32),
-            *[pltpu.VMEM((LAYERS, nz - 1, zrows, depth), BF16)] * 2,
-            pltpu.VMEM((zrows, depth), BF16),
+            pltpu.VMEM((CHUNKS, n, share, wide), F32),
+            pltpu.VMEM((CHUNKS, n, share, wide), BF16),
+            pltpu.VMEM((CHUNKS, n - 1, share, wide), BF16),
+            pltpu.VMEM((CHUNKS, n, n, share, pw), BF16),
+            pltpu.VMEM((LAYERS, CHUNKS, nz, zrows, depth), F32),
+            *[pltpu.VMEM((LAYERS, CHUNKS, nz - 1, zrows, depth), BF16)] * 2,
+            pltpu.VMEM((CHUNKS, zrows, depth), BF16),
             pltpu.VMEM((2, width, depth), BF16),
             dma((7 + n // 2,)),
             *[dma((n - 1,))] * 2,
@@ -395,16 +429,16 @@
             *[dma((1 + n // 2,))] * 2,
             *[dma((2, 2, n))] * 2,
             *[dma((2, n - 1))] * 2,
-            *[dma((n - 1,))] * 2,
-            *[dma((LAYERS, n - 1))] * 2,
-            *[dma((LAYERS, n, n - 1))] * 2,
-            *[dma((LAYERS, nz - 1))] * 2,
-            *[dma((nz, n))] * 2,
-            *[dma((2, nz))] * 2,
+            *[dma((CHUNKS, n - 1))] * 2,
+            *[dma((1 + CHUNKS, n - 1))] * 2,
+            *[dma((1 + CHUNKS, n, n - 1))] * 2,
+            *[dma((LAYERS, CHUNKS, nz - 1))] * 2,
+            *[dma((CHUNKS, nz, n))] * 2,
+            *[dma((CHUNKS, 2, nz))] * 2,
         ]
         result = pl.pallas_call(
             functools.partial(kernel, n, nz, depth * n * n),
-            out_shape=jax.ShapeDtypeStruct((2 * nz, zrows, depth), BF16),
+            out_shape=jax.ShapeDtypeStruct((2, CHUNKS, nz, zrows, depth), BF16),
             in_specs=[pl.BlockSpec(memory_space=pl.ANY)] * 5,
             out_specs=pl.BlockSpec(memory_space=pltpu.VMEM),
             scratch_shapes=scratch,

time: 85.8 us -> 83.8 us (0.977)
  Pallas kernels: 83.7 us -> 82 us
    pallas_call x1, Pallas kernels: 83.7 us -> 82 us  [body(): pl.pallas_call(functools.partial(kernel, n, nz, depth * n * n), out_shape...]
where the time goes in v5:
time: 83.8 us; the launch traced here: 83.7 us
  Pallas kernels  82 us (98%)
  local copies, waits for them, and re-layouts  1.67 us (2%)
    pallas_call x1, Pallas kernels, body(): pl.pallas_call(functools.partial(kernel, n, nz, depth * n * n), out_shape...  82 us

profile of v5, /device:TPU:1, one launch (start us, length us, event | category | flops | bytes accessed | tf_op | source)
XLA Modules:
  0.0 83.7 jit_solution(17228075739084457627)
XLA Ops:
  0.0 82.0 %shard_map.55 = bf16[2,2,8,16,256]{4,3,2,1,0:T(8,128)(2,1)} custom-call(bf16[512,256]{1,0:T(8,128)(2,1)} %tok.1, f32[2,256]{1,0:T(2,128)} %gain.1, bf16[2,704,256]{2,1,0:T(8,128)(2,1)} %bitcast.4, bf16[2,704,256]{2,1,0:T(8,128)(2,1)} %bitcast.5, bf16[2,704,256]{2,1,0:T(8,128)(2,1)} %wd.1), custom_call_target="tpu_custom_call" | custom-call | tf_op jit(solution)/shard_map/pallas_call | solution.py:439
  82.0 1.7 %copy.7 = bf16[512,256]{1,0:T(8,128)(2,1)} copy(bf16[512,256]{1,0:T(8,128)(2,1)} %bitcast.3) | data formatting | bytes 524288

commit v6 on v5

--- a/solution.py
+++ b/solution.py
@@ -266,7 +266,7 @@
             copy.wait_recv()
 
     semaphores = [tuple(s.at[k] for s in (sq, rq, sp, rp)) for k in range(1 + CHUNKS)]
-    for _ in gather(hid0, semaphores[0], 0, nothing, lambda: deal_parts("p")):
+    for _ in gather(hid0, semaphores[0], 0, lambda: deal_parts("q"), lambda: deal_parts("p")):
         pass
     wait_down(0)
 
@@ -289,7 +289,7 @@
         fresh[g] = sum_along_z(0, g, copies, before)
         along = {
             d: send(fresh.at[g], stream.at[g, 0, z], ss.at[g, d, 0], rs.at[g, d, 0], {**z_peer(d), **other})
-            for d in far_first(nz) + [0]
+            for d in [0] + near_first(nz)
         }
         arriving = {}
         for e in [0] + near_first(nz):
@@ -378,7 +378,7 @@
 
 
 CHUNKS = 2
-DEAL = ('p', 'p', 'z', 'z')
+DEAL = ('q', 'p', 'z', 'z')
 
 
 def solution(mesh):

time: 83.8 us -> 82 us (0.979)
  Pallas kernels: 82 us -> 80.2 us
    pallas_call x1, Pallas kernels: 82 us -> 80.2 us  [body(): pl.pallas_call(functools.partial(kernel, n, nz, depth * n * n), out_shape...]
where the time goes in v6:
time: 82 us; the launch traced here: 81.9 us
  Pallas kernels  80.2 us (98%)
  local copies, waits for them, and re-layouts  1.67 us (2%)
    pallas_call x1, Pallas kernels, body(): pl.pallas_call(functools.partial(kernel, n, nz, depth * n * n), out_shape...  80.2 us
    unnamed x1, local copies, waits for them, and re-layouts  1.67 us

profile of v6, /device:TPU:1, one launch (start us, length us, event | category | flops | bytes accessed | tf_op | source)
XLA Modules:
  0.0 81.9 jit_solution(11516513055353793720)
XLA Ops:
  0.0 80.2 %shard_map.55 = bf16[2,2,8,16,256]{4,3,2,1,0:T(8,128)(2,1)} custom-call(bf16[512,256]{1,0:T(8,128)(2,1)} %tok.1, f32[2,256]{1,0:T(2,128)} %gain.1, bf16[2,704,256]{2,1,0:T(8,128)(2,1)} %bitcast.4, bf16[2,704,256]{2,1,0:T(8,128)(2,1)} %bitcast.5, bf16[2,704,256]{2,1,0:T(8,128)(2,1)} %wd.1), custom_call_target="tpu_custom_call" | custom-call | tf_op jit(solution)/shard_map/pallas_call | solution.py:439
  80.2 1.7 %copy.7 = bf16[512,256]{1,0:T(8,128)(2,1)} copy(bf16[512,256]{1,0:T(8,128)(2,1)} %bitcast.3) | data formatting | bytes 524288

commit v7 on v6

--- a/solution.py
+++ b/solution.py
@@ -443,9 +443,9 @@
             out_specs=pl.BlockSpec(memory_space=pltpu.VMEM),
             scratch_shapes=scratch,
             compiler_params=pltpu.CompilerParams(
-                collective_id=0, has_side_effects=True, vmem_limit_bytes=60 * 1024 * 1024
+                collective_id=0, has_side_effects=True, vmem_limit_bytes=24 * 1024 * 1024
             ),
-        )(tokens, norm_gain, jnp.swapaxes(gate_weight, 1, 2), jnp.swapaxes(up_weight, 1, 2), down_weight)
+        )(*(pltpu.with_memory_space_constraint(a, pltpu.HBM) for a in (tokens, norm_gain, jnp.swapaxes(gate_weight, 1, 2), jnp.swapaxes(up_weight, 1, 2), down_weight)))
         return result.reshape(count, depth)
 
     in_specs = (P(None, ra), P(None, ra), P(None, ra, cb), P(None, ra, cb), P(None, cb, ra))

time: 82 us -> 80.5 us (0.982)
  local copies, waits for them, and re-layouts: 1.67 us -> 0.71 us
    unnamed x1, local copies, waits for them, and re-layouts: 1.67 us -> 0.71 us
where the time goes in v7:
time: 80.5 us; the launch traced here: 80.4 us
  Pallas kernels  79.7 us (99%)
    pallas_call x1, Pallas kernels, body(): pl.pallas_call(functools.partial(kernel, n, nz, depth * n * n), out_shape...  79.7 us

profile of v7, /device:TPU:1, one launch (start us, length us, event | category | flops | bytes accessed | tf_op | source)
XLA Modules:
  0.0 80.4 jit_solution(16108094037833821622)
XLA Ops:
  0.0 79.7 %shard_map.55 = bf16[2,2,8,16,256]{4,3,2,1,0:T(8,128)(2,1)S(1)} custom-call(bf16[512,256]{1,0:T(8,128)(2,1)} %tok.1, f32[2,256]{1,0:T(2,128)} %gain.1, bf16[2,704,256]{2,1,0:T(8,128)(2,1)} %bitcast.4, bf16[2,704,256]{2,1,0:T(8,128)(2,1)} %bitcast.5, bf16[2,704,256]{2,1,0:T(8,128)(2,1)} %wd.1), custom_call_target="tpu_custom_call" | custom-call | tf_op jit(solution)/shard_map/pallas_call | solution.py:439
  79.7 0.7 copy.7

commit v8 on v7

--- a/solution.py
+++ b/solution.py
@@ -230,8 +230,8 @@
         across = {d: send(at, at, sq.at[d - 1], rq.at[d - 1], q_peer(d)) for d in far_first(n)}
         spread(0)
         between()
+        yield
         for d in near_first(n):
-            yield
             across[d].wait_recv()
             spread(d)
         after()
@@ -292,8 +292,8 @@
             for d in [0] + near_first(nz)
         }
         arriving = {}
+        yield
         for e in [0] + near_first(nz):
-            yield
             along[e].wait_recv()
             k = lax.rem(z + nz - e, nz)
             for d in far_first(n):

time: 80.5 us -> 78.7 us (0.978)
  Pallas kernels: 79.7 us -> 77.9 us
    pallas_call x1, Pallas kernels: 79.7 us -> 77.9 us  [body(): pl.pallas_call(functools.partial(kernel, n, nz, depth * n * n), out_shape...]
where the time goes in v8:
time: 78.7 us; the launch traced here: 78.6 us
  Pallas kernels  77.9 us (99%)
    pallas_call x1, Pallas kernels, body(): pl.pallas_call(functools.partial(kernel, n, nz, depth * n * n), out_shape...  77.9 us

profile of v8, /device:TPU:1, one launch (start us, length us, event | category | flops | bytes accessed | tf_op | source)
XLA Modules:
  0.0 78.6 jit_solution(3149516487391077343)
XLA Ops:
  0.0 77.9 %shard_map.55 = bf16[2,2,8,16,256]{4,3,2,1,0:T(8,128)(2,1)S(1)} custom-call(bf16[512,256]{1,0:T(8,128)(2,1)} %tok.1, f32[2,256]{1,0:T(2,128)} %gain.1, bf16[2,704,256]{2,1,0:T(8,128)(2,1)} %bitcast.4, bf16[2,704,256]{2,1,0:T(8,128)(2,1)} %bitcast.5, bf16[2,704,256]{2,1,0:T(8,128)(2,1)} %wd.1), custom_call_target="tpu_custom_call" | custom-call | tf_op jit(solution)/shard_map/pallas_call | solution.py:439
  77.9 0.7 copy.7
